TPU v7x, 128 devices: a whole 4x4x4 slice. The times are simulated.
128 devices in a mesh: kv: 16 (over z, x), tp: 8 (over y, core).
Axes of the slice: x: 4, y: 4, z: 4, core: 2. Of those that a mesh axis runs over, the one named last changes fastest.
Arguments:
- tokens: bfloat16 [32768, 2048], P('kv'), may hold values from -6 to 6
- norm_gain: bfloat16 [2048], replicated, may hold values from 0.099609375 to 1.8984375
- query_weight: bfloat16 [2048, 1024], P(None, 'tp'), may hold values from -0.125 to 0.125
- cmp_key_weight: bfloat16 [2048, 512], P(None, 'tp'), may hold values from -0.125 to 0.125
- cmp_value_weight: bfloat16 [2048, 512], P(None, 'tp'), may hold values from -0.125 to 0.125
- sel_key_weight: bfloat16 [2048, 512], P(None, 'tp'), may hold values from -0.125 to 0.125
- sel_value_weight: bfloat16 [2048, 512], P(None, 'tp'), may hold values from -0.125 to 0.125
- branch_weight: bfloat16 [2, 2048, 16], replicated, may hold values from -0.125 to 0.125
- key_embed: bfloat16 [8, 32, 64], P('tp'), may hold values from -3 to 3
- key_inner: bfloat16 [8, 2048, 64], P('tp'), may hold values from -0.125 to 0.125
- key_outer: bfloat16 [8, 64, 64], P('tp'), may hold values from -0.75 to 0.75
- value_embed: bfloat16 [8, 32, 64], P('tp'), may hold values from -3 to 3
- value_inner: bfloat16 [8, 2048, 64], P('tp'), may hold values from -0.125 to 0.125
- value_outer: bfloat16 [8, 64, 64], P('tp'), may hold values from -0.75 to 0.75
- out_weight: bfloat16 [1024, 2048], replicated, may hold values from -0.1875 to 0.1875
- chosen: int32 [8, 256, 8], P('tp'), may hold values from 0 to 511, as said below
Outputs:
- attended: bfloat16 [32768, 2048], P(('kv', 'tp'))
Inputs may be any that keep to these rules, and one draw needn't show every extreme that they name: `chosen`: each entry is the index of a block of 64 positions in the whole sequence. For every key head and query block, its 8 entries lie in 8 different aligned spans of 2048 positions (at most one from any span), and none lies inside the query block's own positions.
All inputs are finite; a program needn't handle non-finite values.
Results may differ from a plain program's by a relative error of at most 0.0075.
Values may be sent and summed in bfloat16 or wider, within the bound.
A program may use at most 128 MiB of HBM per device.

v0:
```python
import jax
import jax.numpy as jnp
from jax import lax
from jax.sharding import PartitionSpec as P

HEAD_DIM = 64
CMP_BLOCK = 32
SEL_BLOCK = 64
Q_BLOCK = 128
FAR_PICKS = 8


ROPE_BASE = 10000.0
norm_eps = 1e-06
masked_score = -1000000000.0


def copy_for_each(x, axis):
    peers = lax.axis_size(axis)
    return lax.all_to_all(jnp.broadcast_to(x[None], (peers, *x.shape)), axis, 0, 0, tiled=True)


def in_order(pieces, dim):
    shape = list(pieces.shape[1:])
    shape[dim] *= pieces.shape[0]
    return jnp.moveaxis(pieces, 0, dim).reshape(shape)


def collect(x, axis, dim):
    pieces = copy_for_each(x, axis)
    return in_order(pieces, dim)


def rotate(values_in, positions):
    half_dim = values_in.shape[-1] // 2
    inverse = ROPE_BASE ** (-jnp.arange(half_dim, dtype=jnp.float32) / half_dim)
    rotary_phases = positions.astype(jnp.float32)[:, None] * inverse[None, :]
    cosine = jnp.cos(rotary_phases)[:, None, :]
    sine = jnp.sin(rotary_phases)[:, None, :]
    first_half = values_in[..., :half_dim]
    second_half = values_in[..., half_dim:]
    return jnp.concatenate(
        [first_half * cosine - second_half * sine, second_half * cosine + first_half * sine],
        axis=-1,
    )


def summarize(raw_rows, embed, inner, outer):
    kv_local = embed.shape[0]
    block_count = raw_rows.shape[0] // CMP_BLOCK
    blocked = (
        raw_rows.reshape(block_count, CMP_BLOCK, kv_local, HEAD_DIM)
        .transpose(2, 0, 1, 3)
        .astype(jnp.float32)
    )
    blocked = (blocked + embed.astype(jnp.float32)[:, None]).astype(jnp.bfloat16)
    blocked = blocked.reshape(kv_local, block_count, CMP_BLOCK * HEAD_DIM)
    hidden = jax.nn.gelu(
        jnp.einsum("knc,kce->kne", blocked, inner, preferred_element_type=jnp.float32)
    ).astype(jnp.bfloat16)
    return jnp.einsum("kne,kef->knf", hidden, outer, preferred_element_type=jnp.float32).astype(
        jnp.bfloat16
    )


def per_device(
    tokens,
    norm_gain,
    query_weight,
    cmp_key_weight,
    cmp_value_weight,
    sel_key_weight,
    sel_value_weight,
    branch_weight,
    key_embed,
    key_inner,
    key_outer,
    value_embed,
    value_inner,
    value_outer,
    out_weight,
    chosen,
):
    tok_rows = tokens.shape[0]
    kv_local = key_embed.shape[0]
    heads_local = query_weight.shape[1] // HEAD_DIM
    group_size = heads_local // kv_local
    owners = lax.axis_size("kv")
    dev_index = lax.axis_index("kv")
    offset = dev_index * tok_rows
    positions = offset + jnp.arange(tok_rows, dtype=jnp.int32)
    scale = HEAD_DIM ** (-0.5)
    expanded_mask = tokens.astype(jnp.float32)
    normed = (
        expanded_mask
        * lax.rsqrt(jnp.mean(expanded_mask * expanded_mask, axis=-1, keepdims=True) + norm_eps)
        * norm_gain.astype(jnp.float32)
    ).astype(jnp.bfloat16)
    gate_cols = lax.dynamic_slice_in_dim(
        branch_weight, lax.axis_index("tp") * heads_local, heads_local, 2
    )
    q_width = heads_local * HEAD_DIM
    kv_width = kv_local * HEAD_DIM
    joined_weight = jnp.concatenate(
        [
            query_weight,
            cmp_key_weight,
            cmp_value_weight,
            sel_key_weight,
            sel_value_weight,
            gate_cols[0],
            gate_cols[1],
        ],
        axis=1,
    )
    projected = jnp.dot(normed, joined_weight, preferred_element_type=jnp.float32)
    bounds = [
        q_width,
        q_width + kv_width,
        q_width + 2 * kv_width,
        q_width + 3 * kv_width,
        q_width + 4 * kv_width,
        q_width + 4 * kv_width + heads_local,
    ]
    (
        query_part,
        cmp_key_part,
        cmp_value_part,
        sel_key_part,
        sel_value_part,
        gate_cmp_part,
        gate_sel_part,
    ) = jnp.split(projected, bounds, axis=1)
    query = query_part.reshape(tok_rows, heads_local, HEAD_DIM)
    q_plain = query.astype(jnp.bfloat16)
    q_turn = rotate(query, positions).astype(jnp.bfloat16)
    cmp_key = cmp_key_part.astype(jnp.bfloat16).reshape(tok_rows, kv_local, HEAD_DIM)
    cmp_value = cmp_value_part.astype(jnp.bfloat16).reshape(tok_rows, kv_local, HEAD_DIM)
    sel_key = rotate(sel_key_part.reshape(tok_rows, kv_local, HEAD_DIM), positions).astype(
        jnp.bfloat16
    )
    selected_value = sel_value_part.astype(jnp.bfloat16).reshape(tok_rows, kv_local, HEAD_DIM)
    gate_cmp = jax.nn.sigmoid(gate_cmp_part)
    gate_sel = jax.nn.sigmoid(gate_sel_part)
    summary = jnp.concatenate(
        [
            summarize(cmp_key, key_embed, key_inner, key_outer),
            summarize(cmp_value, value_embed, value_inner, value_outer),
        ],
        axis=-1,
    )
    summaries = collect(summary, "kv", 1)
    summary_count = summaries.shape[1]
    block_end = (jnp.arange(summary_count, dtype=jnp.int32) + 1) * CMP_BLOCK - 1
    q_group = q_plain.reshape(tok_rows, kv_local, group_size, HEAD_DIM).transpose(1, 0, 2, 3)
    cmp_scores = (
        jnp.einsum(
            "ktgd,kcd->ktgc", q_group, summaries[..., :HEAD_DIM], preferred_element_type=jnp.float32
        )
        * scale
    )
    usable = (block_end[None, :] <= positions[:, None])[None, :, None, :]
    cmp_probs = jax.nn.softmax(
        jnp.where(usable, cmp_scores, masked_score), axis=-1
    ) * usable.astype(jnp.float32)
    out_cmp = jnp.einsum(
        "ktgc,kcd->ktgd",
        cmp_probs.astype(jnp.bfloat16),
        summaries[..., HEAD_DIM:],
        preferred_element_type=jnp.float32,
    )
    out_cmp = out_cmp.transpose(1, 0, 2, 3).reshape(tok_rows, heads_local, HEAD_DIM)
    span_queries = tok_rows // Q_BLOCK
    span_blocks = tok_rows // SEL_BLOCK
    kv_sel = jnp.concatenate([sel_key, selected_value], axis=-1).transpose(1, 0, 2)
    all_picks = chosen.reshape(kv_local, owners, span_queries, FAR_PICKS)
    my_picks = lax.dynamic_index_in_dim(all_picks, dev_index, 1, keepdims=False)
    head_lane = jnp.arange(kv_local, dtype=jnp.int32)[:, None, None]
    matches = all_picks // span_blocks == dev_index
    wanted = jnp.sum(jnp.where(matches, all_picks % span_blocks, 0), axis=3)
    blocked = kv_sel.reshape(kv_local, span_blocks, SEL_BLOCK, 2 * HEAD_DIM)
    outgoing = blocked[head_lane, wanted]
    incoming = lax.all_to_all(outgoing, "kv", split_axis=1, concat_axis=1, tiled=True)
    source = my_picks // span_blocks
    query_lane = jnp.arange(span_queries, dtype=jnp.int32)[None, :, None]
    picked = incoming[head_lane, source, query_lane]
    own_keys = kv_sel.reshape(kv_local, span_queries, Q_BLOCK, 2 * HEAD_DIM)
    keys_all = jnp.concatenate(
        [own_keys, picked.reshape(kv_local, span_queries, FAR_PICKS * SEL_BLOCK, 2 * HEAD_DIM)],
        axis=2,
    )
    query_pos = positions.reshape(span_queries, Q_BLOCK)
    far_pos = (my_picks[..., None] * SEL_BLOCK + jnp.arange(SEL_BLOCK, dtype=jnp.int32)).reshape(
        kv_local, span_queries, FAR_PICKS * SEL_BLOCK
    )
    key_pos = jnp.concatenate([query_pos[None], far_pos], axis=2)
    q_sel = q_turn.reshape(span_queries, Q_BLOCK, kv_local, group_size, HEAD_DIM).transpose(
        2, 0, 1, 3, 4
    )
    sel_scores = (
        jnp.einsum(
            "knqgd,knmd->knqgm", q_sel, keys_all[..., :HEAD_DIM], preferred_element_type=jnp.float32
        )
        * scale
    )
    allowed_keys = key_pos[:, :, None, None, :] <= query_pos[None, :, :, None, None]
    sel_probs = jax.nn.softmax(jnp.where(allowed_keys, sel_scores, masked_score), axis=-1)
    out_sel = jnp.einsum(
        "knqgm,knmd->knqgd",
        sel_probs.astype(jnp.bfloat16),
        keys_all[..., HEAD_DIM:],
        preferred_element_type=jnp.float32,
    )
    out_sel = out_sel.transpose(1, 2, 0, 3, 4).reshape(tok_rows, heads_local, HEAD_DIM)
    mixed = (
        (gate_cmp[..., None] * out_cmp + gate_sel[..., None] * out_sel)
        .reshape(tok_rows, heads_local * HEAD_DIM)
        .astype(jnp.bfloat16)
    )
    head_rows = lax.all_to_all(mixed, "tp", split_axis=0, concat_axis=1, tiled=True)
    return jnp.dot(head_rows, out_weight, preferred_element_type=jnp.float32).astype(jnp.bfloat16)


def solution(mesh):
    placed = (
        P("kv", None),
        P(),
        P(None, "tp"),
        P(None, "tp"),
        P(None, "tp"),
        P(None, "tp"),
        P(None, "tp"),
        P(),
        P("tp", None, None),
        P("tp", None, None),
        P("tp", None, None),
        P("tp", None, None),
        P("tp", None, None),
        P("tp", None, None),
        P(),
        P("tp", None, None),
    )
    return jax.shard_map(
        per_device, mesh=mesh, in_specs=placed, out_specs=P(("kv", "tp"), None), check_vma=False
    )
```

profile of v0, /device:TPU:1, one launch (start us, length us, event | category | flops | bytes accessed | tf_op | source)
XLA Modules:
  0.0 171.9 jit_solution(5051237416359795915)
XLA Ops:
  0.0 0.8 convert_element_type.126
  0.8 5.1 %fusion.2 = f32[2048]{0:T(1024)S(1)} fusion(bf16[2048,2048]{1,0:T(8,128)(2,1)} %param.16), kind=kLoop, calls=%fused_computation.6 | loop fusion | flops 12580864 | bytes 8396800 | tf_op jit(solution)/shard_map/reduce_sum | solution.py:96
  6.0 0.8 dynamic-slice_bitcast_fusion
  6.8 0.3 copy.63
  7.1 0.3 copy.62
  7.4 1.0 copy.58
  8.4 1.0 copy.59
  9.5 1.0 copy.60
  10.5 1.0 copy.61
  11.5 0.1 add.242
  11.6 0.3 copy.66
  11.9 0.1 add.235
  12.1 0.3 copy.64
  12.4 5.5 %concatenate.68 = bf16[2048,388]{1,0:T(8,128)(2,1)} concatenate(bf16[2048,128]{1,0:T(8,128)(2,1)} %param.18, bf16[2048,64]{1,0:T(8,128)(2,1)} %copy.58, bf16[2048,64]{1,0:T(8,128)(2,1)} %copy.59, bf16[2048,64]{1,0:T(8,128)(2,1)} %copy.60, bf16[2048,64]{1,0:T(8,128)(2,1)} %copy.61, bf16[2048,2]{1,0:T(8,128)(2,1)S(1)} %copy.62, bf16[2048,2]{1,0:T(8,128)(2,1)S(1)} %copy.63), dimensions={1} | concatenate | bytes 3178496 | tf_op jit(solution)/shard_map/concatenate | solution.py:104
  17.8 9.4 %fusion.119 = (bf16[2048,388]{0,1:T(8,128)(2,1)S(1)}, f32[2048,388]{0,1:T(8,128)}) fusion(bf16[2048,388]{1,0:T(8,128)(2,1)} %concatenate.68, bf16[2048,2048]{1,0:T(8,128)(2,1)} %param.16, f32[2048]{0:T(1024)S(1)} %convert_element_type.126, f32[2048]{0:T(1024)S(1)} %add_rsqrt_fusion), kind=kOutput, calls=%fused_computation.179 | convolution fusion | flops 3272351744 | bytes 14761984 | tf_op jit(solution)/shard_map/dot_general | solution.py:116
  27.2 0.1 add_convert_fusion.2
  27.4 1.0 copy-done.11
  28.4 0.3 copy.65
  28.7 0.5 convert_element_type.132
  29.1 0.3 copy.67
  29.4 0.5 convert_element_type.138
  29.9 0.4 fusion.23
  30.3 0.4 fusion.24
  30.7 0.8 broadcast_in_dim.34
  31.5 8.5 %all-to-all-start = ((bf16[16,1,64,128]{3,2,1,0:T(8,128)(2,1)}), bf16[16,1,64,128]{3,2,1,0:T(8,128)(2,1)}, u32[]{:S(2)}, u32[]{:S(2)}) async-start(bf16[16,1,64,128]{3,2,1,0:T(8,128)(2,1)} %broadcast_in_dim.34), calls=%async_computation | async-start | bytes 524288 | tf_op jit(solution)/shard_map/all_to_all | solution.py:20
  40.2 1.7 %slice_bitcast_fusion.14 = (bf16[8,8,16,128]{3,1,2,0:T(8,128)(2,1)}, bf16[2048,64]{0,1:T(8,128)(2,1)S(1)}) fusion(bf16[2048,388]{0,1:T(8,128)(2,1)} %copy-done.11), kind=kLoop, calls=%fused_computation.176 | loop fusion | bytes 786432
  41.9 1.6 fusion.78
  43.5 1.1 slice_bitcast_fusion.4
  44.5 1.3 split.34
  46.4 0.3 copy.91
  46.7 1.8 %multiply_cosine_fusion.1 = (f32[2048,32]{0,1:T(8,128)}, f32[2048,32]{0,1:T(8,128)}) fusion(f32[32]{0:T(128)S(1)} %multiply_power_fusion, f32[2048]{0:T(1024)S(1)} %get-tuple-element.30), kind=kLoop, calls=%fused_computation.56 | loop fusion | flops 65536 | bytes 532608 | tf_op jit(solution)/shard_map/cos | solution.py:38
  48.5 1.1 fusion.35
  49.7 0.3 copy.89
  50.0 0.3 copy.90
  50.3 1.8 %broadcast_compare_fusion.1 = pred[16,128,640]{2,1,0:T(8,128)(4,1)} fusion(s32[16,128]{1,0:T(8,128)S(1)} %add_add_fusion, s32[16,640]{1,0:T(8,128)S(1)} %add_bitcast_fusion), kind=kLoop, calls=%fused_computation.30 | loop fusion | flops 1310720 | bytes 1359872 | tf_op jit(solution)/shard_map/le | solution.py:206
  52.0 0.5 pad_maximum_fusion.1
  52.5 3.1 %gather_fusion = bf16[256,64,128]{2,1,0:T(8,128)(2,1)} fusion(bf16[1,32,64,128]{3,2,1,0:T(8,128)(2,1)S(1)} %pad_maximum_fusion.1, s32[256]{0:T(256)S(1)} %reshape.731), kind=kCustom, calls=%fused_computation | custom fusion | bytes 8390656 | tf_op jit(solution)/shard_map/gather | solution.py:182
  55.6 0.2 fusion.38
  55.8 6.8 %all-to-all-start.1 = ((bf16[1,16,16,64,128]{4,3,2,0,1:T(8,128)(2,1)}), bf16[1,16,16,64,128]{4,3,2,0,1:T(8,128)(2,1)}, u32[]{:S(2)}, u32[]{:S(2)}) async-start(bf16[1,16,16,64,128]{4,3,2,0,1:T(8,128)(2,1)} %bitcast.158), calls=%async_computation.1 | async-start | bytes 8388608 | tf_op jit(solution)/shard_map/all_to_all | solution.py:183
  62.6 2.1 %split.57 = bf16[2048,128]{0,1:T(8,128)(2,1)} slice(f32[2048,388]{0,1:T(8,128)} %get-tuple-element.24), slice={[0:2048], [0:128]} | slice | bytes 1048576 | tf_op jit(solution)/shard_map/split | solution.py:133
  64.9 0.8 copy.76
  65.7 0.8 copy.104
  66.5 0.7 copy.74
  67.2 0.8 copy.103
  68.0 0.1 mul.232
  68.1 0.3 copy.97
  68.5 4.2 %fusion.118 = (f32[2048,1024]{0,1:T(8,128)}, pred[2048,1024]{0,1:T(8,128)(4,1)S(1)}) fusion(s32[2048]{0:T(1024)S(1)} %get-tuple-element.29, s32[1024]{0:T(1024)S(1)} %multiply_add_fusion), kind=kLoop, calls=%fused_computation.178 | loop fusion | flops 4194304 | bytes 10498048 | tf_op jit(solution)/shard_map/convert_element_type | solution.py:165
  72.6 10.6 %fusion.121 = (f32[2048,2]{0,1:T(2,128)S(1)}, f32[2048,2,1024]{0,2,1:T(8,128)}) fusion(pred[2048,1024]{0,1:T(8,128)(4,1)S(1)} %get-tuple-element.20, bf16[2048,2,64]{0,2,1:T(8,128)(2,1)} %bitcast.173, bf16[1,1024,128]{2,1,0:T(8,128)(2,1)} %bitcast.14), kind=kOutput, calls=%fused_computation.181 | convolution fusion | flops 553649152 | bytes 19677184 | tf_op jit(solution)/shard_map/sub | solution.py:163
  83.3 9.4 %fusion.19 = f32[2048,2,64]{0,2,1:T(8,128)S(1)} fusion(f32[2048,2,1024]{0,2,1:T(8,128)} %get-tuple-element.28, f32[2048,1024]{0,1:T(8,128)} %get-tuple-element.19, f32[2048,2]{0,1:T(2,128)S(1)} %get-tuple-element.27, f32[2048,2]{0,1:T(2,128)S(1)} %copy-done.20, bf16[1,1024,128]{2,1,0:T(8,128)(2,1)} %bitcast.14), kind=kOutput, calls=%fused_computation.32 | convolution fusion | flops 549715968 | bytes 26509312 | tf_op jit(solution)/shard_map/ktgc,kcd->ktgd/dot_general | solution.py:166
  92.7 1.3 copy.96
  94.0 29.5 %all-to-all-done.1 = bf16[1,16,16,64,128]{4,3,2,0,1:T(8,128)(2,1)} async-done(((bf16[1,16,16,64,128]{4,3,2,0,1:T(8,128)(2,1)}), bf16[1,16,16,64,128]{4,3,2,0,1:T(8,128)(2,1)}, u32[]{:S(2)}, u32[]{:S(2)}) %all-to-all-start.1) | async-done | bytes 4194336 | tf_op jit(solution)/shard_map/all_to_all | solution.py:183
  123.5 4.5 %gather_fusion.1 = bf16[128,64,128]{2,1,0:T(8,128)(2,1)} fusion(bf16[1,16,16,64,128]{4,3,2,1,0:T(8,128)(2,1)} %bitcast.29, s32[128]{0:T(128)S(1)} %reshape.739), kind=kCustom, calls=%fused_computation.1 | custom fusion | bytes 4195840 | tf_op jit(solution)/shard_map/gather | solution.py:186
  127.9 2.9 %copy.83 = bf16[1,16,512,128]{2,3,1,0:T(8,128)(2,1)S(1)} copy(bf16[1,16,512,128]{3,2,1,0:T(8,128)(2,1)} %bitcast.159) | data formatting | bytes 4194304 | tf_op jit(solution)/shard_map/reshape | solution.py:189
  130.9 1.3 pad_maximum_fusion
  132.2 1.6 copy-done.2
  133.8 1.6 fusion.22
  135.4 7.2 %fusion.120 = (f32[16,128,2]{1,2,0:T(2,128)S(1)}, f32[16,128,2,640]{3,1,2,0:T(8,128)}) fusion(f32[16,128,2,640]{3,1,2,0:T(8,128)S(1)} %fusion.22, pred[16,128,640]{2,1,0:T(8,128)(4,1)S(1)} %copy-done.5), kind=kOutput, calls=%fused_computation.180 | output fusion | flops 15729279 | bytes 22298624 | tf_op jit(solution)/shard_map/sub | solution.py:207
  142.5 5.4 %fusion.18 = f32[16,128,2,64]{1,3,2,0:T(8,128)S(1)} fusion(f32[16,128,2,640]{3,1,2,0:T(8,128)} %get-tuple-element.26, f32[16,128,2]{1,2,0:T(2,128)S(1)} %get-tuple-element.25, bf16[1,16,640,128]{2,3,1,0:T(8,128)(2,1)S(1)} %copy-done.3), kind=kOutput, calls=%fused_computation.27 | convolution fusion | flops 340787200 | bytes 12861440 | tf_op jit(solution)/shard_map/knqgm,knmd->knqgd/dot_general | solution.py:208
  148.0 1.6 copy.84
  149.5 2.5 %reshape_transpose.10 = f32[8,256,128]{1,0,2:T(8,128)} reshape(f32[16,128,2,64]{1,0,3,2:T(8,128)} %copy.84) | data formatting | bytes 2097152 | tf_op jit(solution)/shard_map/reshape;transpose | solution.py:214
  152.1 1.6 fusion.26
  153.6 0.1 copy.85
  153.7 15.9 %all_to_all.26 = bf16[8,256,128]{1,2,0:T(8,128)(2,1)S(1)} all-to-all(bf16[8,256,128]{1,2,0:T(8,128)(2,1)S(1)} %copy.85), channel_id=1, replica_groups=mesh['kv'=16,'tp'=8] {'tp'}, dimensions={0} | all-to-all | bytes 1048576 | tf_op jit(solution)/shard_map/all_to_all | solution.py:220
  169.6 2.2 %convolution_convert_fusion = bf16[256,2048]{1,0:T(8,128)(2,1)} fusion(bf16[256,1024]{0,1:T(8,128)(2,1)S(1)} %bitcast.174, bf16[1024,2048]{1,0:T(8,128)(2,1)S(1)} %copy-done.23), kind=kOutput, calls=%fused_computation.31 | convolution fusion | flops 1074266112 | bytes 5767168 | tf_op jit(solution)/shard_map/dot_general | solution.py:221
  (82 shorter events, 1.2 us)
Async XLA Ops:
  0.0 29.9 %copy-start = (bf16[1,2048,64]{1,2,0:T(8,128)(2,1)S(1)}, bf16[1,2048,64]{1,2,0:T(8,128)(2,1)}, u32[]{:S(2)}) copy-start(bf16[1,2048,64]{1,2,0:T(8,128)(2,1)} %param.25) | copy-start | bytes 786436
  0.0 5.9 %copy-start.21 = (bf16[1,32,64]{2,1,0:T(8,128)(2,1)S(1)}, bf16[1,32,64]{2,1,0:T(8,128)(2,1)}, u32[]{:S(2)}) copy-start(bf16[1,32,64]{2,1,0:T(8,128)(2,1)} %param.24) | copy-start | bytes 12292
  0.0 6.0 %copy-start.22 = (bf16[1,32,64]{2,1,0:T(8,128)(2,1)S(1)}, bf16[1,32,64]{2,1,0:T(8,128)(2,1)}, u32[]{:S(2)}) copy-start(bf16[1,32,64]{2,1,0:T(8,128)(2,1)} %param.27) | copy-start | bytes 12292
  0.0 7.4 %copy-start.12 = (bf16[2048,64]{0,1:T(8,128)(2,1)S(1)}, bf16[2048,64]{0,1:T(8,128)(2,1)}, u32[]{:S(2)}) copy-start(bf16[2048,64]{0,1:T(8,128)(2,1)} %param.19) | copy-start | bytes 786436
  0.0 8.4 %copy-start.13 = (bf16[2048,64]{0,1:T(8,128)(2,1)S(1)}, bf16[2048,64]{0,1:T(8,128)(2,1)}, u32[]{:S(2)}) copy-start(bf16[2048,64]{0,1:T(8,128)(2,1)} %param.20) | copy-start | bytes 786436
  0.8 8.7 %copy-start.14 = (bf16[2048,64]{0,1:T(8,128)(2,1)S(1)}, bf16[2048,64]{0,1:T(8,128)(2,1)}, u32[]{:S(2)}) copy-start(bf16[2048,64]{0,1:T(8,128)(2,1)} %param.21) | copy-start | bytes 786436
  0.8 9.7 %copy-start.15 = (bf16[2048,64]{0,1:T(8,128)(2,1)S(1)}, bf16[2048,64]{0,1:T(8,128)(2,1)}, u32[]{:S(2)}) copy-start(bf16[2048,64]{0,1:T(8,128)(2,1)} %param.22) | copy-start | bytes 786436
  27.2 1.2 copy-start.11
  27.2 2.7 %copy-start.18 = (bf16[1,64,64]{2,1,0:T(8,128)(2,1)S(1)}, bf16[1,64,64]{2,1,0:T(8,128)(2,1)}, u32[]{:S(2)}) copy-start(bf16[1,64,64]{2,1,0:T(8,128)(2,1)} %param.26) | copy-start | bytes 24580
  27.2 3.0 %copy-start.16 = (bf16[1,2048,64]{1,2,0:T(8,128)(2,1)S(1)}, bf16[1,2048,64]{1,2,0:T(8,128)(2,1)}, u32[]{:S(2)}) copy-start(bf16[1,2048,64]{1,2,0:T(8,128)(2,1)} %param.28) | copy-start | bytes 786436
  27.2 3.1 %copy-start.19 = (bf16[1,64,64]{2,1,0:T(8,128)(2,1)S(1)}, bf16[1,64,64]{2,1,0:T(8,128)(2,1)}, u32[]{:S(2)}) copy-start(bf16[1,64,64]{2,1,0:T(8,128)(2,1)} %param.29) | copy-start | bytes 24580
  27.2 12.8 %copy-start.17 = (s32[1,256,8]{1,2,0:T(8,128)S(1)}, s32[1,256,8]{1,2,0:T(8,128)}, u32[]{:S(2)}) copy-start(s32[1,256,8]{1,2,0:T(8,128)} %param.31) | copy-start | bytes 24580
  31.5 24.3 %all-to-all-start = ((bf16[16,1,64,128]{3,2,1,0:T(8,128)(2,1)}), bf16[16,1,64,128]{3,2,1,0:T(8,128)(2,1)}, u32[]{:S(2)}, u32[]{:S(2)}) async-start(bf16[16,1,64,128]{3,2,1,0:T(8,128)(2,1)} %broadcast_in_dim.34), calls=%async_computation | async-start | bytes 524288 | tf_op jit(solution)/shard_map/all_to_all | solution.py:20
  52.5 3.1 %copy-start.9 = (f32[2048,32]{0,1:T(8,128)S(1)}, f32[2048,32]{0,1:T(8,128)}, u32[]{:S(2)}) copy-start(f32[2048,32]{0,1:T(8,128)} %get-tuple-element.21) | copy-start | bytes 786436
  52.5 3.1 %copy-start.10 = (f32[2048,32]{0,1:T(8,128)S(1)}, f32[2048,32]{0,1:T(8,128)}, u32[]{:S(2)}) copy-start(f32[2048,32]{0,1:T(8,128)} %get-tuple-element.22) | copy-start | bytes 786436
  55.8 9.1 %copy-start.6 = (bf16[8,8,16,128]{3,1,2,0:T(8,128)(2,1)S(1)}, bf16[8,8,16,128]{3,1,2,0:T(8,128)(2,1)}, u32[]{:S(2)}) copy-start(bf16[8,8,16,128]{3,1,2,0:T(8,128)(2,1)} %get-tuple-element.11) | copy-start | bytes 786436
  55.8 67.7 %all-to-all-start.1 = ((bf16[1,16,16,64,128]{4,3,2,0,1:T(8,128)(2,1)}), bf16[1,16,16,64,128]{4,3,2,0,1:T(8,128)(2,1)}, u32[]{:S(2)}, u32[]{:S(2)}) async-start(bf16[1,16,16,64,128]{4,3,2,0,1:T(8,128)(2,1)} %bitcast.158), calls=%async_computation.1 | async-start | bytes 8388608 | tf_op jit(solution)/shard_map/all_to_all | solution.py:183
  72.6 10.6 %copy-start.20 = (f32[2048,2]{0,1:T(2,128)S(1)}, f32[2048,2]{0,1:T(2,128)}, u32[]{:S(2)}) copy-start(f32[2048,2]{0,1:T(2,128)} %get-tuple-element.7) | copy-start | bytes 49156
  127.9 5.8 %copy-start.7 = (bf16[2,4,16,8,128]{4,3,1,0,2:T(8,128)(2,1)S(1)}, bf16[2,4,16,8,128]{4,3,1,0,2:T(8,128)(2,1)}, u32[]{:S(2)}) copy-start(bf16[2,4,16,8,128]{4,3,1,0,2:T(8,128)(2,1)} %copy.104) | copy-start | bytes 786436
  130.8 2.9 %copy-start.8 = (bf16[2,4,16,8,128]{4,3,1,0,2:T(8,128)(2,1)S(1)}, bf16[2,4,16,8,128]{4,3,1,0,2:T(8,128)(2,1)}, u32[]{:S(2)}) copy-start(bf16[2,4,16,8,128]{4,3,1,0,2:T(8,128)(2,1)} %copy.103) | copy-start | bytes 786436
  132.2 1.6 copy-start.2
  133.8 1.6 copy-start.5
  135.3 7.2 %copy-start.3 = (bf16[1,16,640,128]{2,3,1,0:T(8,128)(2,1)S(1)}, bf16[1,16,640,128]{2,3,1,0:T(8,128)(2,1)}, u32[]{:S(2)}) copy-start(bf16[1,16,640,128]{2,3,1,0:T(8,128)(2,1)} %copy-done.2) | copy-start | bytes 7864324
  142.5 9.5 %copy-start.4 = (f32[16,8,8,256]{3,2,1,0:T(8,128)S(1)}, f32[16,8,8,256]{3,2,1,0:T(8,128)}, u32[]{:S(2)}) copy-start(f32[16,8,8,256]{3,2,1,0:T(8,128)} %copy.96) | copy-start | bytes 3145732
  152.1 17.6 %copy-start.23 = (bf16[1024,2048]{1,0:T(8,128)(2,1)S(1)}, bf16[1024,2048]{1,0:T(8,128)(2,1)}, u32[]{:S(2)}) copy-start(bf16[1024,2048]{1,0:T(8,128)(2,1)} %param.30) | copy-start | bytes 12582916
  152.1 19.8 %copy-start.1 = (bf16[1,2048,64]{1,2,0:T(8,128)(2,1)S(1)}, bf16[1,2048,64]{1,2,0:T(8,128)(2,1)}, u32[]{:S(2)}) copy-start(bf16[1,2048,64]{1,2,0:T(8,128)(2,1)} %param.25) | copy-start | bytes 786436
where the time goes:
time: 173 us; the launch traced here: 172 us
  local copies, waits for them, and re-layouts  44 us (25%)
  matrix products  39.3 us (23%)
  waiting for transfers between devices  29.5 us (17%)
  other arithmetic  27.4 us (16%)
  blocking collectives  15.9 us (9%)
  starting transfers between devices  15.3 us (9%)
    all_to_all x1, waiting for transfers between devices, per_device(): lax.all_to_all(outgoing, 'kv', split_axis=1, concat_axis=1, tiled=True)  29.5 us
    all_to_all x1, blocking collectives, per_device(): lax.all_to_all(mixed, 'tp', split_axis=0, concat_axis=1, tiled=True)  15.9 us
    sub x1, matrix products, per_device(): jax.nn.softmax(jnp.where(usable, cmp_scores, masked_score), axis=-1)  10.6 us
    unnamed x58, local copies, waits for them, and re-layouts  10.2 us
    dot_general x1, matrix products, per_device(): jnp.einsum('ktgc,kcd->ktgd', cmp_probs.astype(jnp.bfloat16), summaries[.....  9.4 us
    dot_general x1, matrix products, per_device(): jnp.dot(normed, joined_weight, preferred_element_type=jnp.float32)  9.36 us
    all_to_all x1, starting transfers between devices, copy_for_each(): lax.all_to_all(jnp.broadcast_to(x[None], (peers, *x.shape)), axis, 0, 0,...  8.48 us
    sub x1, other arithmetic, per_device(): jax.nn.softmax(jnp.where(allowed_keys, sel_scores, masked_score), axis=-1)  7.17 us
  transfers between devices with their start and end apart: 2, of which 1 were waited for; matrix products, arithmetic and copies ran while one was open for 27% of the time, Pallas kernels for 0%

commit v1 on v0

v1 whole, which is shorter than its diff:
```python
import functools

import jax
import jax.numpy as jnp
import numpy as np
from jax import lax
from jax.experimental import pallas as pl
from jax.experimental.pallas import tpu as pltpu
from jax.sharding import PartitionSpec as P

D = 2048
HD = 64
CMP = 32
SEL = 64
QB = 128
TOK = 2048
NQ = TOK // QB
NB = TOK // SEL
EPS = 1e-06
NEG = -1e30
FLOOR = -1e20
TILE = 512
MESH = pl.DeviceIdType.MESH
NT = (((1,), (1,)), ((), ()))
ORDER = ((2, 0), (2, 1), (1, 0), (3, 0), (1, 1), (3, 1), (0, 1), (0, 0))


def angle_tables():
    lane = np.arange(128)
    freq = 10000.0 ** (-(lane % 32) / 32.0)
    sign = np.where(lane % 64 < 32, -1.0, 1.0)
    coarse = np.arange(512)[:, None] * 64.0 * freq
    fine = np.arange(64)[:, None] * freq
    as32 = lambda t: np.asarray(t, np.float32)
    return as32(np.cos(coarse)), as32(np.sin(coarse)), as32(np.cos(fine)), as32(np.sin(fine)), as32(sign[None])


def lanes(shape):
    return lax.broadcasted_iota(jnp.int32, shape, 1)


def gelu(x):
    return 0.5 * x * (1.0 + jnp.tanh(0.7978845608028654 * (x + 0.044715 * (x * x * x))))


def project_kernel(
    tok_ref, gain_ref, wq_ref, wck_ref, wcv_ref, wsk_ref, wsv_ref, bw_ref, ke_ref, ki_ref, ko_ref,
    ve_ref, vi_ref, vo_ref, cc_ref, cs_ref, fc_ref, fs_ref, sg_ref,
    kv_ref, qs_ref, qc_ref, g_ref, sum_ref,
    w_ref, raw_ref,
):
    step = pl.program_id(0)
    tp = lax.axis_index("tp")
    kv = lax.axis_index("kv")

    @pl.when(step == 0)
    def _():
        w_ref[0:64, :] = wsk_ref[...]
        w_ref[64:128, :] = wsv_ref[...]
        w_ref[128:192, :] = wck_ref[...]
        w_ref[192:256, :] = wcv_ref[...]
        w_ref[256:384, :] = wq_ref[...].T
        row = lax.broadcasted_iota(jnp.int32, (128, 16), 0)
        col = lax.broadcasted_iota(jnp.int32, (128, 16), 1)
        e0 = jnp.where((row < 2) & (col == 2 * tp + row), 1.0, 0.0).astype(jnp.bfloat16)
        e1 = jnp.where((row >= 2) & (row < 4) & (col == 2 * tp + row - 2), 1.0, 0.0).astype(jnp.bfloat16)
        picked = jnp.dot(e0, bw_ref[0], preferred_element_type=jnp.float32)
        picked += jnp.dot(e1, bw_ref[1], preferred_element_type=jnp.float32)
        w_ref[384:512, :] = picked.astype(jnp.bfloat16)

    x = tok_ref[...].astype(jnp.float32)
    inv = lax.rsqrt(jnp.mean(x * x, axis=1, keepdims=True) + EPS)
    normed = (x * inv * gain_ref[...].astype(jnp.float32)).astype(jnp.bfloat16)
    proj = lax.dot_general(normed, w_ref[...], NT, preferred_element_type=jnp.float32)
    base = kv * 32 + step * (TILE // 64)
    cosine, sine = [], []
    for u in range(TILE // 64):
        cc = cc_ref[pl.ds(base + u, 1), :]
        cs = cs_ref[pl.ds(base + u, 1), :]
        cosine.append(cc * fc_ref[...] - cs * fs_ref[...])
        sine.append((cs * fc_ref[...] + cc * fs_ref[...]) * sg_ref[...])
    cosine = jnp.concatenate(cosine, axis=0)
    sine = jnp.concatenate(sine, axis=0)
    lane = lanes((TILE, 128))
    front = (lane % 64) < 32
    low = lane < 64

    def turn(v):
        other = jnp.where(front, pltpu.roll(v, 96, 1), pltpu.roll(v, 32, 1))
        return v * cosine + other * sine

    sel = proj[:, 0:128]
    kv_ref[...] = jnp.where(low, turn(sel), sel).astype(jnp.bfloat16)
    raw = proj[:, 128:256].astype(jnp.bfloat16).astype(jnp.float32)
    embed = jnp.concatenate([ke_ref[...], ve_ref[...]], axis=1).astype(jnp.float32)
    raw = raw + jnp.concatenate([embed] * (TILE // CMP), axis=0)
    raw_ref[pl.ds(pl.multiple_of(step * TILE, TILE), TILE), :] = raw.astype(jnp.bfloat16).astype(jnp.float32)
    q = proj[:, 256:384]
    for ref, val in ((qc_ref, q), (qs_ref, turn(q))):
        val = val.astype(jnp.bfloat16).astype(jnp.float32) * 0.125
        ref[0] = jnp.where(low, val, 0.0).astype(jnp.bfloat16)
        ref[1] = jnp.where(low, pltpu.roll(val, 64, 1), 0.0).astype(jnp.bfloat16)
    g_ref[...] = 1.0 / (1.0 + jnp.exp(-proj[:, 384:512]))

    @pl.when(step == TOK // TILE - 1)
    def _():
        keys, values = [], []
        low64 = lanes((64, 128)) < 64
        for r in range(0, CMP, 2):
            one = raw_ref[pl.ds(r, 64, stride=CMP), :]
            two = raw_ref[pl.ds(r + 1, 64, stride=CMP), :]
            keys.append(jnp.where(low64, one, pltpu.roll(two, 64, 1)).astype(jnp.bfloat16))
            values.append(jnp.where(low64, pltpu.roll(one, 64, 1), two).astype(jnp.bfloat16))
        parts = []
        for rows, inner, outer in ((keys, ki_ref, ko_ref), (values, vi_ref, vo_ref)):
            flat = jnp.concatenate(rows, axis=1)
            hidden = lax.dot_general(flat, inner[...], NT, preferred_element_type=jnp.float32)
            hidden = gelu(hidden).astype(jnp.bfloat16)
            parts.append(jnp.dot(hidden, outer[...], preferred_element_type=jnp.float32))
        sum_ref[...] = jnp.concatenate(parts, axis=1).astype(jnp.bfloat16)


def run_project(tokens, gain, wq, wck, wcv, wsk, wsv, bw, ke, ki, ko, ve, vi, vo):
    cc, cs, fc, fs, sg = angle_tables()
    whole = lambda shape: pl.BlockSpec(shape, lambda i: (0,) * len(shape))
    ops = [gain, wq, wck, wcv, wsk, wsv, bw, ke, ki, ko, ve, vi, vo] + [jnp.asarray(t) for t in (cc, cs, fc, fs, sg)]
    return pl.pallas_call(
        project_kernel,
        grid=(TOK // TILE,),
        in_specs=[pl.BlockSpec((TILE, D), lambda i: (i, 0))] + [whole(o.shape) for o in ops],
        out_specs=[
            pl.BlockSpec((TILE, 128), lambda i: (i, 0)),
            pl.BlockSpec((2, TILE, 128), lambda i: (0, i, 0)),
            pl.BlockSpec((2, TILE, 128), lambda i: (0, i, 0)),
            pl.BlockSpec((TILE, 128), lambda i: (i, 0)),
            whole((64, 128)),
        ],
        out_shape=[
            jax.ShapeDtypeStruct((TOK, 128), jnp.bfloat16),
            jax.ShapeDtypeStruct((2, TOK, 128), jnp.bfloat16),
            jax.ShapeDtypeStruct((2, TOK, 128), jnp.bfloat16),
            jax.ShapeDtypeStruct((TOK, 128), jnp.float32),
            jax.ShapeDtypeStruct((64, 128), jnp.bfloat16),
        ],
        scratch_shapes=[pltpu.VMEM((512, D), jnp.bfloat16), pltpu.VMEM((TOK, 128), jnp.float32)],
        compiler_params=pltpu.CompilerParams(vmem_limit_bytes=48 << 20),
        name="project",
    )(tokens, *ops)


def attend_kernel(
    want_ref, bias_ref, kv_ref, summ_ref, qs_ref, qc_ref, g_ref,
    out_ref,
    full1, full2, full3, inb, outb, fwd, sums, acc, mrow, ocmp, mix, hr,
    a_send, a_recv, af_send, af_recv, s_send, s_recv, b_send, b_recv, f_send, f_recv, t_send, t_recv,
):
    full = (kv_ref, full1, full2, full3)
    tp = lax.axis_index("tp")
    kv = lax.axis_index("kv")
    core = lax.rem(tp, 2)
    yy = tp // 2
    zz = kv // 4
    xx = lax.rem(kv, 4)
    sa = 4 - 3 * core
    sb = 1 + 3 * core
    aa = zz * (1 - core) + xx * core
    bb = xx * (1 - core) + zz * core

    def at(r, s):
        return lax.rem(aa + r, 4) * sa + lax.rem(bb + s, 4) * sb

    def tp_at(dy, dc):
        return 2 * lax.rem(yy + dy, 4) + (core + dc - 2 * core * dc)

    def near(r, s):
        return {"kv": at(r, s), "tp": tp}

    barrier = pltpu.get_barrier_semaphore()
    peers = [near(r, 0) for r in (1, 2, 3)] + [near(0, s) for s in (1, 2, 3)]
    peers += [{"kv": kv, "tp": tp_at(*o)} for o in ORDER[:-1]]
    for peer in peers:
        pl.semaphore_signal(barrier, inc=1, device_id=peer, device_id_type=MESH)
    pl.semaphore_wait(barrier, len(peers))

    def remote(src, dst, ssem, rsem, dev):
        return pltpu.make_async_remote_copy(
            src_ref=src, dst_ref=dst, send_sem=ssem, recv_sem=rsem, device_id=dev, device_id_type=MESH
        )

    started = []

    def go(copy):
        copy.start()
        started.append(copy)

    sums[0, 0] = summ_ref[...]
    for r in (1, 2, 3):
        go(remote(summ_ref, sums.at[0, 4 - r], s_send.at[r - 1], s_recv.at[3 - r], near(r, 0)))
    half = NB // 2
    for h in (0, 1):
        for r, slot, part in ((1, 3, h), (3, 1, 1 - h)):
            rows = pl.ds(part * half, half)
            i = (slot // 2) * 2 + part
            go(remote(kv_ref.at[rows], full[slot].at[rows], a_send.at[i], a_recv.at[i], near(r, 0)))

    def a_wait(slot, part):
        rows = pl.ds(part * half, half)
        i = (slot // 2) * 2 + part
        remote(kv_ref.at[rows], full[slot].at[rows], a_send.at[i], a_recv.at[i], near(1, 0)).wait_recv()

    def a_forward(slot, part, r, i):
        rows = pl.ds(part * half, half)
        go(remote(full[slot].at[rows], full[2].at[rows], af_send.at[i], af_recv.at[i], near(r, 0)))

    def af_wait(i):
        rows = pl.ds(i * half, half)
        remote(full[0].at[rows], full[2].at[rows], af_send.at[i], af_recv.at[i], near(1, 0)).wait_recv()

    def order_of(c):
        return [tp_at(*o) for o in ORDER][c]

    def q_of(i):
        c = i // 2
        dest = 0
        for k in range(8):
            dest = dest + jnp.where(c == k, tp_at(*ORDER[k]), 0)
        return dest * 2 + lax.rem(i, 2)

    def select(r):
        span = at(r, 0)
        dests = [at(0, s) for s in range(4)]

        def body(i, _):
            q = q_of(i)
            for s in range(4):
                blk = want_ref[span * 256 + dests[s] * 16 + q]
                val = full[r][blk]
                if s == 0:
                    inb[r, 0, i] = val
                else:
                    outb[r, s - 1, i] = val
            return 0

        lax.fori_loop(0, NQ, body, 0)

    def b_start(r):
        go(remote(outb.at[r, 1, pl.ds(0, 8)], fwd.at[r, 0], f_send.at[r, 0], f_recv.at[r, 0], near(0, 1)))
        go(remote(outb.at[r, 1, pl.ds(8, 8)], fwd.at[r, 1], f_send.at[r, 1], f_recv.at[r, 1], near(0, 3)))
        go(remote(outb.at[r, 0], inb.at[r, 3], b_send.at[r, 0], b_recv.at[r, 0], near(0, 1)))
        go(remote(outb.at[r, 2], inb.at[r, 1], b_send.at[r, 1], b_recv.at[r, 1], near(0, 3)))

    def b_forward(r):
        for k, s in ((0, 1), (1, 3)):
            remote(outb.at[r, 1, pl.ds(8 * k, 8)], fwd.at[r, k], f_send.at[r, k], f_recv.at[r, k], near(0, 1)).wait_recv()
            go(remote(fwd.at[r, k], inb.at[r, 2, pl.ds(8 * k, 8)], b_send.at[r, 2 + k], b_recv.at[r, 2 + k], near(0, s)))

    def b_wait(r):
        remote(outb.at[r, 0], inb.at[r, 3], b_send.at[r, 0], b_recv.at[r, 0], near(0, 1)).wait_recv()
        remote(outb.at[r, 2], inb.at[r, 1], b_send.at[r, 1], b_recv.at[r, 1], near(0, 1)).wait_recv()
        for k in (0, 1):
            remote(fwd.at[r, k], inb.at[r, 2, pl.ds(8 * k, 8)], b_send.at[r, 2 + k], b_recv.at[r, 2 + k], near(0, 1)).wait_recv()

    def with_ones(keys):
        return jnp.where(lanes(keys.shape) < HD, jnp.ones_like(keys), keys)

    def scores(q2, keys):
        return lax.dot_general(q2, keys, NT, preferred_element_type=jnp.float32)

    def spread(col):
        return jnp.broadcast_to(col, (2 * QB, 128))

    def weigh(s, m, keys):
        p = jnp.concatenate([jnp.exp(s[:, k:k + 128] - m) for k in range(0, s.shape[1], 128)], axis=1)
        return jnp.dot(p.astype(jnp.bfloat16), with_ones(keys), preferred_element_type=jnp.float32)

    def stacked(ref, q):
        rows = pl.ds(pl.multiple_of(q * QB, QB), QB)
        return jnp.concatenate([ref[0, rows, :], ref[1, rows, :]], axis=0)

    def own_block(i, _):
        q = q_of(i)
        keys = kv_ref[pl.ds(2 * q, 2)].reshape(QB, 128)
        s = scores(stacked(qs_ref, q), keys)
        row = lax.rem(lax.broadcasted_iota(jnp.int32, s.shape, 0), QB)
        s = jnp.where(lanes(s.shape) <= row, s, NEG)
        m = spread(jnp.max(s, axis=1, keepdims=True))
        mrow[i] = m
        acc[i] = weigh(s, m, keys)
        return 0

    def far_step(i, r):
        q = q_of(i)
        keys = inb[r, :, i].reshape(4 * SEL, 128)
        s = scores(stacked(qs_ref, q), keys) + bias_ref[pl.ds(q, 1), r * 256:(r + 1) * 256]
        old = mrow[i]
        m = jnp.maximum(old, spread(jnp.max(s, axis=1, keepdims=True)))
        return m, acc[i] * jnp.exp(old - m) + weigh(s, m, keys)

    def far(r):
        def body(i, _):
            m, a = far_step(i, r)
            mrow[i] = m
            acc[i] = a
            return 0

        lax.fori_loop(0, NQ, body, 0)

    def heads_of(top, bottom):
        low = lanes((QB, 128)) < HD
        num = jnp.where(low, pltpu.roll(top, HD, 1), bottom)
        den = jnp.where(low, top, pltpu.roll(bottom, HD, 1))
        return num, den

    def compressed(i, _):
        q = q_of(i)
        q2 = stacked(qc_ref, q)
        pos = kv * TOK + q * QB + lax.rem(lax.broadcasted_iota(jnp.int32, (2 * QB, 128), 0), QB)
        m = jnp.full((2 * QB, 128), FLOOR, jnp.float32)
        ss = []
        for s in range(4):
            keys = sums[s].reshape(4 * 64, 128)
            sc = scores(q2, keys)
            lane = lanes((1, 256))
            r = lane // 64
            span = lax.rem(aa + r, 4) * sa + lax.rem(bb + s, 4) * sb
            end = span * TOK + (lax.rem(lane, 64) + 1) * CMP - 1
            sc = jnp.concatenate(
                [jnp.where(end[:, k:k + 128] <= pos, sc[:, k:k + 128], NEG) for k in (0, 128)], axis=1
            )
            ss.append(sc)
            m = jnp.maximum(m, jnp.maximum(sc[:, :128], sc[:, 128:]))
        m = spread(jnp.maximum(jnp.max(m, axis=1, keepdims=True), FLOOR))
        total = jnp.zeros((2 * QB, 128), jnp.float32)
        for s in range(4):
            total += weigh(ss[s], m, sums[s].reshape(4 * 64, 128))
        num, den = heads_of(total[:QB], total[QB:])
        ocmp[pl.ds(pl.multiple_of(i * QB, QB), QB), :] = jnp.where(den > 0, num / jnp.maximum(den, 1e-30), 0.0)
        return 0

    def finish(i, r):
        q = q_of(i)
        m, a = far_step(i, r)
        num, den = heads_of(a[:QB], a[QB:])
        rows = pl.ds(pl.multiple_of(q * QB, QB), QB)
        g = g_ref[rows, :]
        low = lanes((QB, 128)) < HD
        gc = jnp.where(low, g[:, 0:1], g[:, 1:2])
        gs = jnp.where(low, g[:, 2:3], g[:, 3:4])
        return gc * ocmp[pl.ds(pl.multiple_of(i * QB, QB), QB), :] + gs * (num / den)

    select(0)
    lax.fori_loop(0, NQ, own_block, 0)
    for r in (1, 2, 3):
        remote(summ_ref, sums.at[0, 4 - r], s_send.at[r - 1], s_recv.at[3 - r], near(r, 0)).wait_recv()
    for s in (1, 2, 3):
        go(remote(sums.at[0], sums.at[4 - s], s_send.at[2 + s], s_recv.at[6 - s], near(0, s)))
    b_start(0)
    for s in (1, 2, 3):
        remote(sums.at[0], sums.at[4 - s], s_send.at[2 + s], s_recv.at[6 - s], near(0, s)).wait_recv()
    lax.fori_loop(0, 4, compressed, 0)
    a_wait(3, 0)
    a_forward(3, 0, 1, 0)
    a_wait(1, 1)
    a_forward(1, 1, 3, 1)
    lax.fori_loop(4, 8, compressed, 0)
    b_forward(0)
    lax.fori_loop(8, 12, compressed, 0)
    a_wait(3, 1)
    select(3)
    b_start(3)
    a_wait(1, 0)
    select(1)
    b_start(1)
    lax.fori_loop(12, 16, compressed, 0)
    af_wait(0)
    af_wait(1)
    select(2)
    b_start(2)
    b_wait(0)
    far(0)
    b_forward(3)
    b_forward(1)
    b_wait(3)
    far(3)
    b_forward(2)
    b_wait(1)
    far(1)
    b_wait(2)
    for c in range(8):
        for k in (0, 1):
            mix[c, k * QB:(k + 1) * QB, :] = finish(2 * c + k, 2).astype(jnp.bfloat16)
        if c < 7:
            go(remote(mix.at[c], hr.at[tp], t_send.at[c], t_recv.at[c], {"kv": kv, "tp": order_of(c)}))
        else:
            hr[tp] = mix[7]
    for c in range(7):
        dy, dc = ORDER[c]
        src = tp_at(4 - dy if dy else 0, dc)
        remote(mix.at[c], hr.at[src], t_send.at[c], t_recv.at[c], {"kv": kv, "tp": order_of(c)}).wait_recv()
    for t in range(8):
        out_ref[:, t * 128:(t + 1) * 128] = hr[t]
    for copy in started:
        copy.wait_send()


def run_attend(want, bias, kvrows, summ, qs, qc, g):
    vm = pl.BlockSpec(memory_space=pltpu.VMEM)
    bf = jnp.bfloat16
    dma = pltpu.SemaphoreType.DMA
    return pl.pallas_call(
        attend_kernel,
        in_specs=[pl.BlockSpec(memory_space=pltpu.SMEM)] + [vm] * 6,
        out_specs=vm,
        out_shape=jax.ShapeDtypeStruct((256, 1024), bf),
        scratch_shapes=[
            pltpu.VMEM((NB, SEL, 128), bf),
            pltpu.VMEM((NB, SEL, 128), bf),
            pltpu.VMEM((NB, SEL, 128), bf),
            pltpu.VMEM((4, 4, NQ, SEL, 128), bf),
            pltpu.VMEM((4, 3, NQ, SEL, 128), bf),
            pltpu.VMEM((4, 2, 8, SEL, 128), bf),
            pltpu.VMEM((4, 4, 64, 128), bf),
            pltpu.VMEM((NQ, 2 * QB, 128), jnp.float32),
            pltpu.VMEM((NQ, 2 * QB, 128), jnp.float32),
            pltpu.VMEM((TOK, 128), jnp.float32),
            pltpu.VMEM((8, 256, 128), bf),
            pltpu.VMEM((8, 256, 128), bf),
            dma((4,)), dma((4,)), dma((2,)), dma((2,)), dma((6,)), dma((6,)),
            dma((4, 4)), dma((4, 4)), dma((4, 2)), dma((4, 2)), dma((8,)), dma((8,)),
        ],
        compiler_params=pltpu.CompilerParams(
            collective_id=0, has_side_effects=True, vmem_limit_bytes=56 << 20
        ),
        name="attend",
    )(want, bias, kvrows, summ, qs, qc, g)


def pick_tables(chosen):
    tp = lax.axis_index("tp")
    kv = lax.axis_index("kv")
    core = tp % 2
    sa, sb = 4 - 3 * core, 1 + 3 * core
    aa = jnp.where(core == 0, kv // 4, kv % 4)
    bb = jnp.where(core == 0, kv % 4, kv // 4)
    picks = chosen[0].T
    span = picks // NB
    match = span[None] == jnp.arange(16, dtype=jnp.int32)[:, None, None]
    want = jnp.sum(jnp.where(match, (picks % NB)[None], 0), axis=1).reshape(4096)
    mine = lax.dynamic_slice_in_dim(chosen[0], kv * NQ, NQ, 0)
    col = jnp.arange(1024, dtype=jnp.int32)
    where_from = ((aa + col // 256) % 4) * sa + ((bb + (col // 64) % 4) % 4) * sb
    start = (kv * NQ + jnp.arange(NQ, dtype=jnp.int32)) * (QB // SEL)
    good = (mine // NB)[:, :, None] == where_from[None, None, :]
    good = good & (mine < start[:, None])[:, :, None]
    bias = jnp.where(jnp.any(good, axis=1), 0.0, NEG).astype(jnp.float32)
    return want, bias


def per_device(
    tokens, norm_gain, query_weight, cmp_key_weight, cmp_value_weight, sel_key_weight, sel_value_weight,
    branch_weight, key_embed, key_inner, key_outer, value_embed, value_inner, value_outer, out_weight, chosen,
):
    want, bias = pick_tables(chosen)
    kvrows, qs, qc, g, summ = run_project(
        tokens, norm_gain.reshape(1, D), query_weight, cmp_key_weight.T, cmp_value_weight.T, sel_key_weight.T,
        sel_value_weight.T, branch_weight.transpose(0, 2, 1), key_embed[0], key_inner[0].T, key_outer[0],
        value_embed[0], value_inner[0].T, value_outer[0],
    )
    rows = run_attend(want, bias, kvrows.reshape(NB, SEL, 128), summ, qs, qc, g)
    return jnp.dot(rows, out_weight, preferred_element_type=jnp.float32).astype(jnp.bfloat16)


def solution(mesh):
    placed = (
        P("kv", None), P(), P(None, "tp"), P(None, "tp"), P(None, "tp"), P(None, "tp"), P(None, "tp"), P(),
        P("tp", None, None), P("tp", None, None), P("tp", None, None), P("tp", None, None),
        P("tp", None, None), P("tp", None, None), P(), P("tp", None, None),
    )
    return jax.shard_map(
        per_device, mesh=mesh, in_specs=placed, out_specs=P(("kv", "tp"), None), check_vma=False
    )
```

time: 173 us -> 110 us (0.64)
  Pallas kernels: 0 us -> 82.7 us
  matrix products: 39.3 us -> 3.27 us
  waiting for transfers between devices: 29.5 us -> 0 us
  local copies, waits for them, and re-layouts: 44 us -> 19.4 us
  other arithmetic: 27.4 us -> 3.2 us
  blocking collectives: 15.9 us -> 0 us
  starting transfers between devices: 15.3 us -> 0 us
    pallas_call x0 -> x2, Pallas kernels: none -> 82.7 us  [the longest x1 70.3 us: run_attend(): pl.pallas_call(attend_kernel, in_specs=[pl.BlockSpec(memory_space=pltpu.S...]
    all_to_all x2 -> x0, waiting for transfers between devices: 29.5 us -> none  [the longest x1 29.5 us: per_device(): lax.all_to_all(outgoing, 'kv', split_axis=1, concat_axis=1, tiled=True)]
    dot_general x7 -> x1, matrix products: 28.7 us -> 3.27 us  [per_device(): jnp.dot(rows, out_weight, preferred_element_type=jnp.float32)]
    all_to_all x1 -> x0, blocking collectives: 15.9 us -> none  [per_device(): lax.all_to_all(mixed, 'tp', split_axis=0, concat_axis=1, tiled=True)]
    all_to_all x2 -> x0, starting transfers between devices: 15.3 us -> none  [the longest x1 8.48 us: copy_for_each(): lax.all_to_all(jnp.broadcast_to(x[None], (peers, *x.shape)), axis, 0, 0,...]
    sub x1 -> x0, matrix products: 10.6 us -> none  [per_device(): jax.nn.softmax(jnp.where(usable, cmp_scores, masked_score), axis=-1)]
    concatenate x13 -> x0, local copies, waits for them, and re-layouts: 9.58 us -> none  [the longest x1 5.46 us: per_device(): jnp.concatenate([query_weight, cmp_key_weight, cmp_value_weight, sel_key_...]
    unnamed x58 -> x45, local copies, waits for them, and re-layouts: 10.2 us -> 18.5 us
  transfers between devices with their start and end apart: 2 -> 0, of which waited for: 1 -> 0; matrix products, arithmetic and copies ran while one was open for 27% -> 0% of each run, Pallas kernels for 0% -> 0%
where the time goes in v1:
time: 110 us; the launch traced here: 109 us
  Pallas kernels  82.7 us (75%)
  local copies, waits for them, and re-layouts  19.4 us (18%)
  matrix products  3.27 us (3%)
  other arithmetic  3.2 us (3%)
    pallas_call x1, Pallas kernels, run_attend(): pl.pallas_call(attend_kernel, in_specs=[pl.BlockSpec(memory_space=pltpu.S...  70.3 us
    unnamed x45, local copies, waits for them, and re-layouts  18.5 us
    pallas_call x1, Pallas kernels, run_project(): pl.pallas_call(project_kernel, grid=(TOK // TILE,), in_specs=[pl.BlockSpe...  12.4 us
    dot_general x1, matrix products, per_device(): jnp.dot(rows, out_weight, preferred_element_type=jnp.float32)  3.27 us

profile of v1, /device:TPU:1, one launch (start us, length us, event | category | flops | bytes accessed | tf_op | source)
XLA Modules:
  0.0 108.6 jit_solution(1916941072585500453)
XLA Ops:
  0.0 0.8 bitcast_compare_fusion.1
  0.8 0.1 copy.25
  0.9 0.8 add_select_fusion.7
  1.6 0.1 copy.24
  1.7 0.2 and_reduce_fusion
  2.0 0.7 reshape.124.gain_ref
  2.7 0.7 add_select_fusion.1
  3.4 0.6 copy.26
  4.0 0.7 broadcast_select_fusion.bias_ref
  4.7 0.0 copy-start.2
  4.7 1.0 copy-done.2
  5.7 0.0 copy-start.4
  5.7 0.9 copy-done.4
  6.7 0.0 copy-start.5
  6.7 0.9 copy-done.5
  7.6 0.0 copy-start.6
  7.6 0.9 copy-done.6
  8.6 0.0 copy-start.7
  8.6 0.9 copy-done.7
  9.5 0.0 copy-start.8
  9.5 0.9 copy-done.8
  10.5 0.0 copy-start.9
  10.5 0.9 copy-done.9
  11.4 0.0 copy-start.10
  11.4 0.9 copy-done.10
  12.4 0.0 copy-start.11
  12.4 0.9 copy-done.11
  13.3 0.0 copy-start.12
  13.3 0.9 copy-done.12
  14.2 0.0 copy-start.13
  14.2 0.8 copy-done.13
  15.0 0.0 copy-start.14
  15.0 0.8 copy-done.14
  15.8 0.0 copy-start.15
  15.8 0.7 copy-done.15
  16.5 0.0 copy-start.16
  16.5 0.7 copy-done.16
  17.2 0.0 copy-start.18
  17.2 0.7 copy-done.18
  17.9 0.0 copy-start.19
  17.9 0.7 copy-done.19
  18.6 0.0 copy-start.20
  18.6 0.7 copy-done.20
  19.2 12.4 %project.1 = (bf16[2048,128]{1,0:T(8,128)(2,1)S(1)}, bf16[2,2048,128]{2,1,0:T(8,128)(2,1)S(1)}, bf16[2,2048,128]{2,1,0:T(8,128)(2,1)S(1)}, f32[2048,128]{1,0:T(8,128)}, bf16[64,128]{1,0:T(8,128)(2,1)S(1)}) custom-call(bf16[2048,2048]{1,0:T(8,128)(2,1)} %tok_ref.1, bf16[1,2048]{1,0:T(2,128)(2,1)S(1)} %reshape.124.gain_ref, bf16[2048,128]{1,0:T(8,128)(2,1)S(1)} %copy-done.2, ...), custom_call_target="tpu_custom_call" | custom-call | tf_op jit(solution)/shard_map/project/pallas_call | solution.py:127
  31.7 0.0 copy-start
  31.7 1.0 copy-done
  32.6 0.0 copy-start.1
  32.6 1.0 copy-done.1
  33.6 0.0 copy-start.3
  33.6 0.8 copy-done.3
  34.4 0.0 copy-start.17
  34.4 0.6 copy-done.17
  35.0 0.0 copy-start.21
  35.0 70.3 %attend.1 = bf16[256,1024]{1,0:T(8,128)(2,1)} custom-call(s32[4096]{0:T(1024)} %bitcast.77, f32[16,1024]{1,0:T(8,128)} %broadcast_select_fusion.bias_ref, bf16[32,64,128]{2,1,0:T(8,128)(2,1)} %bitcast.65, bf16[64,128]{1,0:T(8,128)(2,1)} %copy-done.17, bf16[2,2048,128]{2,1,0:T(8,128)(2,1)} %copy-done, bf16[2,2048,128]{2,1,0:T(8,128)(2,1)} %copy-done.1, ...), custom_call_target="tpu_custom_call" | custom-call | tf_op jit(solution)/shard_map/attend/pallas_call | solution.py:410
  105.3 0.0 copy-done.21
  105.3 3.3 %convolution_convert_fusion = bf16[256,2048]{1,0:T(8,128)(2,1)} fusion(bf16[256,1024]{1,0:T(8,128)(2,1)} %attend.1, bf16[1024,2048]{1,0:T(8,128)(2,1)S(1)} %copy-done.21), kind=kOutput, calls=%fused_computation | convolution fusion | flops 1074266112 | bytes 5767168 | tf_op jit(solution)/shard_map/dot_general | solution.py:470
  (3 shorter events, 0.1 us)
Async XLA Ops:
  4.7 1.0 copy-start.2
  5.7 0.9 copy-start.4
  6.7 0.9 copy-start.5
  7.6 0.9 copy-start.6
  8.6 0.9 copy-start.7
  9.5 0.9 copy-start.8
  10.5 0.9 copy-start.9
  11.4 0.9 copy-start.10
  12.4 0.9 copy-start.11
  13.3 0.9 copy-start.12
  14.2 0.8 copy-start.13
  15.0 0.8 copy-start.14
  15.8 0.7 copy-start.15
  16.5 0.7 copy-start.16
  17.2 0.7 copy-start.18
  17.9 0.7 copy-start.19
  18.6 0.7 copy-start.20
  31.7 1.0 copy-start
  32.6 1.0 copy-start.1
  33.6 0.8 copy-start.3
  34.4 0.6 copy-start.17
  35.0 70.3 %copy-start.21 = (bf16[1024,2048]{1,0:T(8,128)(2,1)S(1)}, bf16[1024,2048]{1,0:T(8,128)(2,1)}, u32[]{:S(2)}) copy-start(bf16[1024,2048]{1,0:T(8,128)(2,1)} %param.35) | copy-start | bytes 12582916

commit v2 on v0

v2 whole, which is shorter than its diff:
```python
import jax
import jax.numpy as jnp
import numpy as np
from jax import lax
from jax.experimental import pallas as pl
from jax.experimental.pallas import tpu as pltpu
from jax.sharding import PartitionSpec as P

D = 2048
HD = 64
CMP = 32
SEL = 64
QB = 128
TOK = 2048
NQ = TOK // QB
NB = TOK // SEL
EPS = 1e-06
NEG = -1e30
FLOOR = -1e20
TILE = 512
MESH = pl.DeviceIdType.MESH
NT = (((1,), (1,)), ((), ()))
BF = jnp.bfloat16
F32 = jnp.float32
ORDER = ((2, 0), (2, 1), (1, 0), (3, 0), (1, 1), (3, 1), (0, 1), (0, 0))


def angle_tables():
    lane = np.arange(128)
    freq = 10000.0 ** (-(lane % 32) / 32.0)
    sign = np.where(lane % 64 < 32, -1.0, 1.0)
    coarse = np.arange(512)[:, None] * 64.0 * freq
    fine = np.arange(64)[:, None] * freq
    as32 = lambda t: jnp.asarray(np.asarray(t, np.float32))
    return as32(np.cos(coarse)), as32(np.sin(coarse)), as32(np.cos(fine)), as32(np.sin(fine)), as32(sign[None])


def lanes(shape):
    return lax.broadcasted_iota(jnp.int32, shape, 1)


def rows_of(shape):
    return lax.broadcasted_iota(jnp.int32, shape, 0)


def gelu(x):
    return 0.5 * x * (1.0 + jnp.tanh(0.7978845608028654 * (x + 0.044715 * (x * x * x))))


def kernel(
    tab, gain_ref, ke_ref, ko_ref, ve_ref, vo_ref, fc_ref, fs_ref, sg_ref,
    tok_hbm, wq_hbm, wck_hbm, wcv_hbm, wsk_hbm, wsv_hbm, bw_hbm, ki_hbm, vi_hbm, cc_hbm, cs_hbm, ow_hbm,
    out_hbm,
    tok, wst, w1, wqv, bwv, w2, kiv, viv, ccv, csv, ow, inv_s, cos_s, sin_s, raw, qs, qc, gt,
    kvb, full1, full2, full3, inb, outb, fwd, own, sums, vtc, acc, mrow, ocmp, mix, hr, res,
    l_sem, a_send, a_recv, af_send, af_recv, s_send, s_recv, b_send, b_recv, f_send, f_recv, t_send, t_recv, o_sem,
):
    full = (kvb, full1, full2, full3)
    tp = lax.axis_index("tp")
    kv = lax.axis_index("kv")
    core = lax.rem(tp, 2)
    yy = tp // 2
    zz = kv // 4
    xx = lax.rem(kv, 4)
    sa = 4 - 3 * core
    sb = 1 + 3 * core
    aa = zz * (1 - core) + xx * core
    bb = xx * (1 - core) + zz * core

    def at(r, s):
        return lax.rem(aa + r, 4) * sa + lax.rem(bb + s, 4) * sb

    def tp_at(dy, dc):
        return 2 * lax.rem(yy + dy, 4) + (core + dc - 2 * core * dc)

    def near(r, s):
        return {"kv": at(r, s), "tp": tp}

    local = []

    def fetch(src, dst):
        copy = pltpu.make_async_copy(src, dst, l_sem.at[len(local)])
        copy.start()
        local.append(copy)
        return copy

    w_in = [fetch(h, wst.at[pl.ds(64 * k, 64)]) for k, h in enumerate((wsk_hbm, wsv_hbm, wck_hbm, wcv_hbm))]
    tiles = TOK // TILE

    def tok_in(t):
        return fetch(tok_hbm.at[pl.ds(t * TILE, TILE)], tok.at[pl.ds(t * TILE, TILE)])

    t_in = [tok_in(0)]
    base = pl.ds(pl.multiple_of(kv * 32, 32), 32)
    a_in = [fetch(cc_hbm.at[base], ccv), fetch(cs_hbm.at[base], csv)]
    t_in += [tok_in(1), tok_in(2), tok_in(3)]
    q_in = [fetch(wq_hbm, wqv), fetch(bw_hbm, bwv)]
    i_in = [fetch(ki_hbm, kiv), fetch(vi_hbm, viv)]
    ow_in = fetch(ow_hbm, ow)

    barrier = pltpu.get_barrier_semaphore()
    peers = [near(r, 0) for r in (1, 2, 3)] + [near(0, s) for s in (1, 2, 3)]
    peers += [{"kv": kv, "tp": tp_at(*o)} for o in ORDER[:-1]]
    for peer in peers:
        pl.semaphore_signal(barrier, inc=1, device_id=peer, device_id_type=MESH)

    started = []

    def remote(src, dst, ssem, rsem, dev):
        return pltpu.make_async_remote_copy(
            src_ref=src, dst_ref=dst, send_sem=ssem, recv_sem=rsem, device_id=dev, device_id_type=MESH
        )

    def go(copy):
        copy.start()
        started.append(copy)

    half = NB // 2

    def a_copy(slot, part, r):
        rows = pl.ds(part * half, half)
        i = (slot // 2) * 2 + part
        return remote(kvb.at[rows], full[slot].at[rows], a_send.at[i], a_recv.at[i], near(r, 0))

    def af_copy(slot, part, r):
        rows = pl.ds(part * half, half)
        return remote(full[slot].at[rows], full2.at[rows], af_send.at[part], af_recv.at[part], near(r, 0))

    gain = gain_ref[...].astype(F32).reshape(1, D)
    for copy in w_in:
        copy.wait()
    for k in range(0, 256, 64):
        w1[k:k + 64, :] = (wst[k:k + 64, :].astype(F32) * gain).astype(BF)
    low = lanes((QB, 128)) < HD
    low64 = lanes((64, 128)) < HD
    front = (lanes((QB, 128)) % 64) < 32

    def turn(v, rows):
        other = jnp.where(front, pltpu.roll(v, 96, 1), pltpu.roll(v, 32, 1))
        return v * cos_s[rows, :] + other * sin_s[rows, :]

    embed = jnp.concatenate([ke_ref[...], ve_ref[...]], axis=1).astype(F32)
    embed = jnp.concatenate([embed] * (QB // CMP), axis=0)
    for t in range(tiles):
        t_in[t].wait()
        if t == 0:
            for copy in a_in:
                copy.wait()
        rows = pl.ds(t * TILE, TILE)
        x = tok[rows, :]
        proj = lax.dot_general(x, w1[...], NT, preferred_element_type=F32)
        xf = x.astype(F32)
        inv = lax.rsqrt(jnp.mean(xf * xf, axis=1, keepdims=True) + EPS)
        inv = jnp.broadcast_to(inv, (TILE, 128))
        inv_s[rows, :] = inv
        for j in range(TILE // QB):
            part = pl.ds(t * TILE + j * QB, QB)
            for u in (0, 1):
                g = t * (TILE // 64) + 2 * j + u
                cc, cs = ccv[g:g + 1, :], csv[g:g + 1, :]
                cos_s[pl.ds(g * 64, 64), :] = cc * fc_ref[...] - cs * fs_ref[...]
                sin_s[pl.ds(g * 64, 64), :] = (cs * fc_ref[...] + cc * fs_ref[...]) * sg_ref[...]
            scale = inv[j * QB:(j + 1) * QB]
            sel = proj[j * QB:(j + 1) * QB, 0:128] * scale
            sel = jnp.where(low, turn(sel, part), sel)
            vt = sel.T[64:128]
            b = t * (TILE // SEL) + 2 * j
            kvb[b] = jnp.where(low64, sel[0:64], pltpu.roll(vt, 64, 1)).astype(BF)
            kvb[b + 1] = jnp.where(low64, sel[64:128], vt).astype(BF)
            val = (proj[j * QB:(j + 1) * QB, 128:256] * scale).astype(BF).astype(F32) + embed
            raw[part, :] = val.astype(BF).astype(F32)
        if t % 2 == 1:
            if t == 1:
                pl.semaphore_wait(barrier, len(peers))
            for slot, r in ((3, 1), (1, 3)):
                go(a_copy(slot, t // 2, r))

    for copy in i_in:
        copy.wait()
    keys, values = [], []
    for r in range(0, CMP, 2):
        one = raw[pl.ds(r, 64, stride=CMP), :]
        two = raw[pl.ds(r + 1, 64, stride=CMP), :]
        keys.append(jnp.where(low64, one, pltpu.roll(two, 64, 1)).astype(BF))
        values.append(jnp.where(low64, pltpu.roll(one, 64, 1), two).astype(BF))
    parts = []
    for rows, inner, outer in ((keys, kiv, ko_ref), (values, viv, vo_ref)):
        flat = jnp.concatenate(rows, axis=1)
        hidden = gelu(lax.dot_general(flat, inner[...], NT, preferred_element_type=F32)).astype(BF)
        parts.append(jnp.dot(hidden, outer[...], preferred_element_type=F32))
    both = jnp.concatenate(parts, axis=1)
    own[...] = jnp.where(low64, both, jnp.concatenate([both, both], axis=0).T[64:128]).astype(BF)
    sums[0, 0] = own[...]

    def s_copy(r):
        return remote(own, sums.at[0, 4 - r], s_send.at[r - 1], s_recv.at[3 - r], near(r, 0))

    def s_bundle(s):
        return remote(sums.at[0], sums.at[4 - s], s_send.at[2 + s], s_recv.at[6 - s], near(0, s))

    for r in (1, 2, 3):
        go(s_copy(r))

    def dest_of(c):
        dest = 0
        for k in range(8):
            dest = dest + jnp.where(c == k, tp_at(*ORDER[k]), 0)
        return dest

    def select(r, g):
        span = at(r, 0)
        dests = [at(0, s) for s in range(4)]

        def body(c, _):
            q0 = dest_of(c) * 2
            for k in (0, 1):
                for s in range(4):
                    blk = tab[span, dests[s] * 16 + q0 + k] & (NB - 1)
                    val = full[r][blk]
                    if s == 0:
                        inb[r, 0, 2 * c + k] = val
                    else:
                        outb[r, s - 1, 2 * c + k] = val
            return 0

        lax.fori_loop(4 * g, 4 * g + 4, body, 0)

    def f_copy(r, g, k):
        part = pl.ds(8 * g + 4 * k, 4)
        return remote(
            outb.at[r, 1, part], fwd.at[r, g, k], f_send.at[r, 2 * g + k], f_recv.at[r, 2 * g + k],
            near(0, 1 + 2 * k),
        )

    def b_copy(r, g, k):
        part = pl.ds(8 * g, 8)
        return remote(
            outb.at[r, 2 * k, part], inb.at[r, 3 - 2 * k, part], b_send.at[r, g, k], b_recv.at[r, g, k],
            near(0, 1 + 2 * k),
        )

    def bf_copy(r, g, k):
        part = pl.ds(8 * g + 4 * k, 4)
        return remote(
            fwd.at[r, g, k], inb.at[r, 2, part], b_send.at[r, g, 2 + k], b_recv.at[r, g, 2 + k],
            near(0, 1 + 2 * k),
        )

    def b_start(r, g):
        for k in (0, 1):
            go(f_copy(r, g, k))
        for k in (0, 1):
            go(b_copy(r, g, k))

    def b_forward(r, g):
        for k in (0, 1):
            f_copy(r, g, k).wait_recv()
            go(bf_copy(r, g, k))

    def b_wait(r, g):
        for k in (0, 1):
            b_copy(r, g, k).wait_recv()
            bf_copy(r, g, k).wait_recv()

    select(0, 0)
    select(0, 1)

    for copy in q_in:
        copy.wait()
    w2[0:128, :] = (wqv[...].T.astype(F32) * gain).astype(BF)
    row = rows_of((128, 16))
    col = lanes((128, 16))
    e0 = jnp.where((row < 2) & (col == 2 * tp + row), 1.0, 0.0).astype(BF)
    e1 = jnp.where((row >= 2) & (row < 4) & (col == 2 * tp + row - 2), 1.0, 0.0).astype(BF)
    picked = jnp.dot(e0, bwv[0], preferred_element_type=F32) + jnp.dot(e1, bwv[1], preferred_element_type=F32)
    w2[128:256, :] = (picked * gain).astype(BF)
    zero = jnp.zeros((64, 256), BF)

    def queries(t):
        rows = pl.ds(t * TILE, TILE)
        proj = lax.dot_general(tok[rows, :], w2[...], NT, preferred_element_type=F32)
        for j in range(TILE // QB):
            part = pl.ds(t * TILE + j * QB, QB)
            q = t * (TILE // QB) + j
            scale = inv_s[part, :]
            v = proj[j * QB:(j + 1) * QB, 0:128] * scale
            for ref, val in ((qc, v), (qs, turn(v, part))):
                val = (val.T.astype(BF).astype(F32) * 0.125).astype(BF)
                ref[q, 0:64, 0:128] = val[0:64]
                ref[q, 0:64, 128:256] = val[64:128]
                ref[q, 64:128, :] = zero
            g = proj[j * QB:(j + 1) * QB, 128:256] * scale
            gt[q] = 1.0 / (1.0 + jnp.exp(-g.T[0:8]))

    queries(0)
    queries(1)
    for r in (1, 2, 3):
        s_copy(r).wait_recv()
    for s in (1, 2, 3):
        go(s_bundle(s))
    b_start(0, 0)
    b_start(0, 1)
    queries(2)
    queries(3)

    def values_of(blocks):
        pairs = [
            jnp.concatenate([blocks[k][:, HD:], blocks[k + 1][:, HD:]], axis=1) for k in range(0, len(blocks), 2)
        ]
        vt = jnp.concatenate(pairs, axis=1)
        return jnp.concatenate([vt, jnp.ones((16, vt.shape[1]), BF)], axis=0)

    def top(s):
        return jnp.max(s, axis=0, keepdims=True)

    def own_block(c, _):
        q0 = dest_of(c) * 2
        for k in (0, 1):
            q, i = q0 + k, 2 * c + k
            blocks = [kvb[2 * q], kvb[2 * q + 1]]
            s = jnp.dot(jnp.concatenate(blocks, axis=0), qs[q], preferred_element_type=F32)
            s = jnp.where(rows_of(s.shape) <= (lanes(s.shape) & (QB - 1)), s, NEG)
            m = top(s)
            mrow[i] = m
            acc[i] = jnp.dot(values_of(blocks), jnp.exp(s - m).astype(BF), preferred_element_type=F32)
        return 0

    def far_step(q, i, r):
        blocks = [inb[r, s, i] for s in range(4)]
        sc = jnp.dot(jnp.concatenate(blocks, axis=0), qs[q], preferred_element_type=F32)
        m = old = mrow[i]
        bias = []
        for s in range(4):
            used = lax.shift_right_logical(tab[at(r, s), kv * 16 + q], 6)
            bias.append((used.astype(F32) - 1.0) * 1e30)
            m = jnp.maximum(m, top(sc[64 * s:64 * s + 64]) + bias[s])
        p = [jnp.exp(sc[64 * s:64 * s + 64] - (m - bias[s])).astype(BF) for s in range(4)]
        add = jnp.dot(values_of(blocks), jnp.concatenate(p, axis=0), preferred_element_type=F32)
        return m, acc[i] * jnp.exp(old - m) + add

    def far(r, g):
        def body(c, _):
            q0 = dest_of(c) * 2
            new = [far_step(q0 + k, 2 * c + k, r) for k in (0, 1)]
            for k in (0, 1):
                mrow[2 * c + k] = new[k][0]
                acc[2 * c + k] = new[k][1]
            return 0

        lax.fori_loop(4 * g, 4 * g + 4, body, 0)

    def compressed(c, _):
        q0 = dest_of(c) * 2
        for k in (0, 1):
            q, i = q0 + k, 2 * c + k
            scs, ms = [], []
            m = jnp.full((1, 256), FLOOR, F32)
            for s in range(4):
                sc = jnp.dot(sums[s].reshape(256, 128), qc[q], preferred_element_type=F32)
                for r in range(4):
                    one = sc[64 * r:64 * r + 64]
                    bias = jnp.where(at(r, s) < kv, 0.0, NEG)
                    if r == 0 and s == 0:
                        end = (rows_of(one.shape) + 1) * CMP - 1
                        one = jnp.where(end <= q * QB + (lanes(one.shape) & (QB - 1)), one, NEG)
                        bias = 0.0
                    scs.append(one)
                    ms.append(bias)
                    m = jnp.maximum(m, top(one) + bias)
            total = jnp.zeros((80, 256), F32)
            for s in range(4):
                p = [jnp.exp(scs[4 * s + r] - (m - ms[4 * s + r])).astype(BF) for r in range(4)]
                total += jnp.dot(
                    vtc[:, 256 * s:256 * s + 256], jnp.concatenate(p, axis=0), preferred_element_type=F32
                )
            den = total[64:65]
            ocmp[i] = jnp.where(den > 0, total[0:64] / jnp.maximum(den, 1e-30), 0.0)
        return 0

    def finish(c):
        q0 = tp_at(*ORDER[c]) * 2
        for k in (0, 1):
            q, i = q0 + k, 2 * c + k
            _, a = far_step(q, i, 2)
            o = a[0:64] / a[64:65]
            oc = ocmp[i]
            g = gt[q]
            heads = [
                g[h:h + 1] * oc[:, 128 * h:128 * h + 128] + g[2 + h:3 + h] * o[:, 128 * h:128 * h + 128]
                for h in (0, 1)
            ]
            mix[c, k * QB:(k + 1) * QB, :] = jnp.concatenate(heads, axis=0).T.astype(BF)

    def t_copy(c, slot):
        return remote(mix.at[c], hr.at[slot], t_send.at[c], t_recv.at[c], {"kv": kv, "tp": tp_at(*ORDER[c])})

    lax.fori_loop(0, 8, own_block, 0)
    for s in (1, 2, 3):
        s_bundle(s).wait_recv()
    for s in range(4):
        vtc[:, 256 * s:256 * s + 256] = values_of([sums[s, r] for r in range(4)])
    lax.fori_loop(0, 2, compressed, 0)
    a_copy(3, 0, 1).wait_recv()
    go(af_copy(3, 0, 1))
    lax.fori_loop(2, 4, compressed, 0)
    b_forward(0, 0)
    a_copy(1, 1, 1).wait_recv()
    go(af_copy(1, 1, 3))
    a_copy(3, 1, 1).wait_recv()
    select(3, 0)
    b_start(3, 0)
    a_copy(1, 0, 1).wait_recv()
    select(1, 0)
    b_start(1, 0)
    b_forward(0, 1)
    select(3, 1)
    select(1, 1)
    lax.fori_loop(4, 6, compressed, 0)
    af_copy(3, 0, 1).wait_recv()
    af_copy(1, 1, 1).wait_recv()
    select(2, 0)
    b_start(2, 0)
    b_start(3, 1)
    b_start(1, 1)
    select(2, 1)
    b_start(2, 1)
    lax.fori_loop(6, 8, compressed, 0)
    b_forward(3, 0)
    b_forward(1, 0)
    b_wait(0, 0)
    far(0, 0)
    b_forward(2, 0)
    b_wait(0, 1)
    far(0, 1)
    b_wait(3, 0)
    far(3, 0)
    b_forward(3, 1)
    b_wait(1, 0)
    far(1, 0)
    b_forward(1, 1)
    b_wait(2, 0)
    for c in range(4):
        finish(c)
        go(t_copy(c, tp))
    b_forward(2, 1)
    b_wait(3, 1)
    far(3, 1)
    b_wait(1, 1)
    far(1, 1)
    b_wait(2, 1)
    for c in range(4, 7):
        finish(c)
        go(t_copy(c, tp))
    finish(7)
    hr[tp] = mix[7]

    ow_in.wait()
    for c in range(7):
        dy, dc = ORDER[c]
        t_copy(c, tp_at((4 - dy) % 4, dc)).wait_recv()
    x = jnp.concatenate([hr[t] for t in range(8)], axis=1)
    outs = []
    for n in range(4):
        cols = pl.ds(n * 512, 512)
        res[:, cols] = jnp.dot(x, ow[:, cols], preferred_element_type=F32).astype(BF)
        copy = pltpu.make_async_copy(res.at[:, cols], out_hbm.at[:, cols], o_sem.at[n])
        copy.start()
        outs.append(copy)
    for copy in started:
        copy.wait_send()
    for copy in outs:
        copy.wait()


def pick_table(chosen):
    picks = chosen[0].T
    block = jnp.arange(256, dtype=jnp.int32)[None, :]
    code = (picks & (NB - 1)) + jnp.where(picks < 2 * block, 64, 0)
    match = (picks >> 5)[None] == jnp.arange(16, dtype=jnp.int32)[:, None, None]
    return jnp.sum(jnp.where(match, code[None], 0), axis=1)


def per_device(
    tokens, norm_gain, query_weight, cmp_key_weight, cmp_value_weight, sel_key_weight, sel_value_weight,
    branch_weight, key_embed, key_inner, key_outer, value_embed, value_inner, value_outer, out_weight, chosen,
):
    cc, cs, fc, fs, sg = angle_tables()
    vm = pl.BlockSpec(memory_space=pltpu.VMEM)
    hbm = pl.BlockSpec(memory_space=pl.ANY)
    dma = pltpu.SemaphoreType.DMA
    v = pltpu.VMEM
    return pl.pallas_call(
        kernel,
        in_specs=[pl.BlockSpec(memory_space=pltpu.SMEM)] + [vm] * 8 + [hbm] * 12,
        out_specs=hbm,
        out_shape=jax.ShapeDtypeStruct((256, D), BF),
        scratch_shapes=[
            v((TOK, D), BF), v((256, D), BF), v((256, D), BF), v((D, 128), BF), v((2, 16, D), BF), v((256, D), BF),
            v((64, D), BF), v((64, D), BF), v((32, 128), F32), v((32, 128), F32), v((1024, D), BF),
            v((TOK, 128), F32), v((TOK, 128), F32), v((TOK, 128), F32), v((TOK, 128), F32),
            v((NQ, 128, 256), BF), v((NQ, 128, 256), BF), v((NQ, 8, 128), F32),
            v((NB, SEL, 128), BF), v((NB, SEL, 128), BF), v((NB, SEL, 128), BF), v((NB, SEL, 128), BF),
            v((4, 4, NQ, SEL, 128), BF), v((4, 3, NQ, SEL, 128), BF), v((4, 2, 2, 4, SEL, 128), BF),
            v((64, 128), BF), v((4, 4, 64, 128), BF), v((80, 1024), BF),
            v((NQ, 80, 256), F32), v((NQ, 1, 256), F32), v((NQ, 64, 256), F32),
            v((8, 256, 128), BF), v((8, 256, 128), BF), v((256, D), BF),
            dma((16,)), dma((4,)), dma((4,)), dma((2,)), dma((2,)), dma((6,)), dma((6,)),
            dma((4, 2, 4)), dma((4, 2, 4)), dma((4, 4)), dma((4, 4)), dma((8,)), dma((8,)), dma((4,)),
        ],
        compiler_params=pltpu.CompilerParams(collective_id=0, has_side_effects=True, vmem_limit_bytes=67043328),
        name="layer",
    )(
        pick_table(chosen), norm_gain, key_embed[0], key_outer[0], value_embed[0], value_outer[0], fc, fs, sg,
        tokens, query_weight, cmp_key_weight.T, cmp_value_weight.T, sel_key_weight.T, sel_value_weight.T,
        branch_weight.transpose(0, 2, 1), key_inner[0].T, value_inner[0].T, cc, cs, out_weight,
    )


def solution(mesh):
    placed = (
        P("kv", None), P(), P(None, "tp"), P(None, "tp"), P(None, "tp"), P(None, "tp"), P(None, "tp"), P(),
        P("tp", None, None), P("tp", None, None), P("tp", None, None), P("tp", None, None),
        P("tp", None, None), P("tp", None, None), P(), P("tp", None, None),
    )
    return jax.shard_map(
        per_device, mesh=mesh, in_specs=placed, out_specs=P(("kv", "tp"), None), check_vma=False
    )
```

time: 173 us -> 78.4 us (0.45)
  Pallas kernels: 0 us -> 74.4 us
  local copies, waits for them, and re-layouts: 44 us -> 2.3 us
  matrix products: 39.3 us -> 0 us
  waiting for transfers between devices: 29.5 us -> 0 us
  other arithmetic: 27.4 us -> 1.35 us
  blocking collectives: 15.9 us -> 0 us
  starting transfers between devices: 15.3 us -> 0 us
    pallas_call x0 -> x1, Pallas kernels: none -> 74.4 us  [per_device(): pl.pallas_call(kernel, in_specs=[pl.BlockSpec(memory_space=pltpu.SMEM)] +...]
    all_to_all x2 -> x0, waiting for transfers between devices: 29.5 us -> none  [the longest x1 29.5 us: per_device(): lax.all_to_all(outgoing, 'kv', split_axis=1, concat_axis=1, tiled=True)]
    dot_general x7 -> x0, matrix products: 28.7 us -> none  [the longest x1 9.4 us: per_device(): jnp.einsum('ktgc,kcd->ktgd', cmp_probs.astype(jnp.bfloat16), summaries[.....]
    all_to_all x1 -> x0, blocking collectives: 15.9 us -> none  [per_device(): lax.all_to_all(mixed, 'tp', split_axis=0, concat_axis=1, tiled=True)]
    all_to_all x2 -> x0, starting transfers between devices: 15.3 us -> none  [the longest x1 8.48 us: copy_for_each(): lax.all_to_all(jnp.broadcast_to(x[None], (peers, *x.shape)), axis, 0, 0,...]
    sub x1 -> x0, matrix products: 10.6 us -> none  [per_device(): jax.nn.softmax(jnp.where(usable, cmp_scores, masked_score), axis=-1)]
    concatenate x13 -> x0, local copies, waits for them, and re-layouts: 9.58 us -> none  [the longest x1 5.46 us: per_device(): jnp.concatenate([query_weight, cmp_key_weight, cmp_value_weight, sel_key_...]
    unnamed x58 -> x1, local copies, waits for them, and re-layouts: 10.2 us -> 2.3 us
  transfers between devices with their start and end apart: 2 -> 0, of which waited for: 1 -> 0; matrix products, arithmetic and copies ran while one was open for 27% -> 0% of each run, Pallas kernels for 0% -> 0%
where the time goes in v2:
time: 78.4 us; the launch traced here: 78.1 us
  Pallas kernels  74.4 us (95%)
  local copies, waits for them, and re-layouts  2.3 us (3%)
  other arithmetic  1.35 us (2%)
    pallas_call x1, Pallas kernels, per_device(): pl.pallas_call(kernel, in_specs=[pl.BlockSpec(memory_space=pltpu.SMEM)] +...  74.4 us
    unnamed x1, local copies, waits for them, and re-layouts  2.3 us

profile of v2, /device:TPU:1, one launch (start us, length us, event | category | flops | bytes accessed | tf_op | source)
XLA Modules:
  0.0 78.1 jit_solution(17362090440092237460)
XLA Ops:
  0.0 0.7 fusion
  0.7 0.6 select_reduce_fusion.tab
  1.4 74.4 %layer.1 = bf16[256,2048]{1,0:T(8,128)(2,1)} custom-call(s32[16,256]{1,0:T(8,128)} %select_reduce_fusion.tab, bf16[2048]{0:T(1024)(128)(2,1)} %gain_ref.1, bf16[32,64]{1,0:T(8,128)(2,1)} %bitcast.40, bf16[64,64]{1,0:T(8,128)(2,1)} %bitcast.38, bf16[32,64]{1,0:T(8,128)(2,1)} %bitcast.41, bf16[64,64]{1,0:T(8,128)(2,1)} %bitcast.39, ...), custom_call_target="tpu_custom_call" | custom-call | tf_op jit(solution)/shard_map/layer/pallas_call | solution.py:492
  75.8 2.3 %copy.23 = bf16[256,2048]{1,0:T(8,128)(2,1)} copy(bf16[256,2048]{1,0:T(8,128)(2,1)} %layer.1) | data formatting | bytes 2097152
  (1 shorter events, 0.0 us)

commit v3 on v2

--- a/solution.py
+++ b/solution.py
@@ -246,11 +246,17 @@
             near(0, 1 + 2 * k),
         )
 
-    def b_start(r, g):
+    def f_start(r, g):
         for k in (0, 1):
             go(f_copy(r, g, k))
+
+    def d_start(r, g):
         for k in (0, 1):
             go(b_copy(r, g, k))
+
+    def b_start(r, g):
+        f_start(r, g)
+        d_start(r, g)
 
     def b_forward(r, g):
         for k in (0, 1):
@@ -300,6 +306,8 @@
         go(s_bundle(s))
     b_start(0, 0)
     b_start(0, 1)
+    a_copy(3, 0, 1).wait_recv()
+    go(af_copy(3, 0, 1))
     queries(2)
     queries(3)
 
@@ -313,41 +321,57 @@
     def top(s):
         return jnp.max(s, axis=0, keepdims=True)
 
-    def own_block(c, _):
-        q0 = dest_of(c) * 2
-        for k in (0, 1):
-            q, i = q0 + k, 2 * c + k
-            blocks = [kvb[2 * q], kvb[2 * q + 1]]
-            s = jnp.dot(jnp.concatenate(blocks, axis=0), qs[q], preferred_element_type=F32)
-            s = jnp.where(rows_of(s.shape) <= (lanes(s.shape) & (QB - 1)), s, NEG)
-            m = top(s)
+    def own_group(g):
+        ids = [(tp_at(*ORDER[c]) * 2 + k, 2 * c + k) for c in range(4 * g, 4 * g + 4) for k in (0, 1)]
+        blocks = [[kvb[2 * q], kvb[2 * q + 1]] for q, _ in ids]
+        scs = [
+            jnp.dot(jnp.concatenate(blk, axis=0), qs[q], preferred_element_type=F32)
+            for blk, (q, _) in zip(blocks, ids)
+        ]
+        ps = []
+        for sc, (_, i) in zip(scs, ids):
+            sc = jnp.where(rows_of(sc.shape) <= (lanes(sc.shape) & (QB - 1)), sc, NEG)
+            m = top(sc)
             mrow[i] = m
-            acc[i] = jnp.dot(values_of(blocks), jnp.exp(s - m).astype(BF), preferred_element_type=F32)
-        return 0
-
-    def far_step(q, i, r):
-        blocks = [inb[r, s, i] for s in range(4)]
-        sc = jnp.dot(jnp.concatenate(blocks, axis=0), qs[q], preferred_element_type=F32)
-        m = old = mrow[i]
-        bias = []
-        for s in range(4):
-            used = lax.shift_right_logical(tab[at(r, s), kv * 16 + q], 6)
-            bias.append((used.astype(F32) - 1.0) * 1e30)
-            m = jnp.maximum(m, top(sc[64 * s:64 * s + 64]) + bias[s])
-        p = [jnp.exp(sc[64 * s:64 * s + 64] - (m - bias[s])).astype(BF) for s in range(4)]
-        add = jnp.dot(values_of(blocks), jnp.concatenate(p, axis=0), preferred_element_type=F32)
-        return m, acc[i] * jnp.exp(old - m) + add
-
-    def far(r, g):
-        def body(c, _):
-            q0 = dest_of(c) * 2
-            new = [far_step(q0 + k, 2 * c + k, r) for k in (0, 1)]
-            for k in (0, 1):
-                mrow[2 * c + k] = new[k][0]
-                acc[2 * c + k] = new[k][1]
+            ps.append(jnp.exp(sc - m).astype(BF))
+        for p, blk, (_, i) in zip(ps, blocks, ids):
+            acc[i] = jnp.dot(values_of(blk), p, preferred_element_type=F32)
+
+    def far_steps(ids, r):
+        blocks = [[inb[r, s, i] for s in range(4)] for _, i in ids]
+        scs = [
+            jnp.dot(jnp.concatenate(blk, axis=0), qs[q], preferred_element_type=F32)
+            for blk, (q, _) in zip(blocks, ids)
+        ]
+        ms, ps, scale = [], [], []
+        for sc, (q, i) in zip(scs, ids):
+            m = old = mrow[i]
+            bias = []
+            for s in range(4):
+                used = lax.shift_right_logical(tab[at(r, s), kv * 16 + q], 6)
+                bias.append((used.astype(F32) - 1.0) * 1e30)
+                m = jnp.maximum(m, top(sc[64 * s:64 * s + 64]) + bias[s])
+            p = [jnp.exp(sc[64 * s:64 * s + 64] - (m - bias[s])).astype(BF) for s in range(4)]
+            ms.append(m)
+            ps.append(jnp.concatenate(p, axis=0))
+            scale.append(jnp.exp(old - m))
+        adds = [jnp.dot(values_of(blk), p, preferred_element_type=F32) for blk, p in zip(blocks, ps)]
+        return ms, [acc[i] * sc + add for (_, i), sc, add in zip(ids, scale, adds)]
+
+    def ids_of(c0, n):
+        return [(tp_at(*ORDER[c]) * 2 + k, 2 * c + k) for c in range(c0, c0 + n) for k in (0, 1)]
+
+    def far_group(g):
+        ids = ids_of(4 * g, 4)
+
+        def body(n, _):
+            ms, accs = far_steps(ids, n + n // 2)
+            for (_, i), m, a in zip(ids, ms, accs):
+                mrow[i] = m
+                acc[i] = a
             return 0
 
-        lax.fori_loop(4 * g, 4 * g + 4, body, 0)
+        lax.fori_loop(0, 3, body, 0)
 
     def compressed(c, _):
         q0 = dest_of(c) * 2
@@ -377,11 +401,10 @@
             ocmp[i] = jnp.where(den > 0, total[0:64] / jnp.maximum(den, 1e-30), 0.0)
         return 0
 
-    def finish(c):
-        q0 = tp_at(*ORDER[c]) * 2
-        for k in (0, 1):
-            q, i = q0 + k, 2 * c + k
-            _, a = far_step(q, i, 2)
+    def finish(c0, n):
+        ids = ids_of(c0, n)
+        _, accs = far_steps(ids, 2)
+        for (q, i), a in zip(ids, accs):
             o = a[0:64] / a[64:65]
             oc = ocmp[i]
             g = gt[q]
@@ -389,69 +412,59 @@
                 g[h:h + 1] * oc[:, 128 * h:128 * h + 128] + g[2 + h:3 + h] * o[:, 128 * h:128 * h + 128]
                 for h in (0, 1)
             ]
-            mix[c, k * QB:(k + 1) * QB, :] = jnp.concatenate(heads, axis=0).T.astype(BF)
+            mix[i // 2, (i % 2) * QB:(i % 2 + 1) * QB, :] = jnp.concatenate(heads, axis=0).T.astype(BF)
 
     def t_copy(c, slot):
         return remote(mix.at[c], hr.at[slot], t_send.at[c], t_recv.at[c], {"kv": kv, "tp": tp_at(*ORDER[c])})
 
-    lax.fori_loop(0, 8, own_block, 0)
+    own_group(0)
+    own_group(1)
+    a_copy(1, 1, 1).wait_recv()
+    go(af_copy(1, 1, 3))
     for s in (1, 2, 3):
         s_bundle(s).wait_recv()
     for s in range(4):
         vtc[:, 256 * s:256 * s + 256] = values_of([sums[s, r] for r in range(4)])
     lax.fori_loop(0, 2, compressed, 0)
-    a_copy(3, 0, 1).wait_recv()
-    go(af_copy(3, 0, 1))
+    a_copy(3, 1, 1).wait_recv()
+    a_copy(1, 0, 1).wait_recv()
+    for r in (3, 1):
+        select(r, 0)
+        f_start(r, 0)
+    for r in (3, 1):
+        select(r, 1)
+        f_start(r, 1)
+    d_start(3, 0)
+    d_start(1, 0)
+    b_forward(0, 0)
+    b_forward(0, 1)
     lax.fori_loop(2, 4, compressed, 0)
-    b_forward(0, 0)
-    a_copy(1, 1, 1).wait_recv()
-    go(af_copy(1, 1, 3))
-    a_copy(3, 1, 1).wait_recv()
-    select(3, 0)
-    b_start(3, 0)
-    a_copy(1, 0, 1).wait_recv()
-    select(1, 0)
-    b_start(1, 0)
-    b_forward(0, 1)
-    select(3, 1)
-    select(1, 1)
-    lax.fori_loop(4, 6, compressed, 0)
     af_copy(3, 0, 1).wait_recv()
     af_copy(1, 1, 1).wait_recv()
-    select(2, 0)
-    b_start(2, 0)
-    b_start(3, 1)
-    b_start(1, 1)
-    select(2, 1)
-    b_start(2, 1)
-    lax.fori_loop(6, 8, compressed, 0)
+    for g in (0, 1):
+        select(2, g)
+        f_start(2, g)
     b_forward(3, 0)
     b_forward(1, 0)
-    b_wait(0, 0)
-    far(0, 0)
+    d_start(2, 0)
+    lax.fori_loop(4, 6, compressed, 0)
     b_forward(2, 0)
-    b_wait(0, 1)
-    far(0, 1)
-    b_wait(3, 0)
-    far(3, 0)
     b_forward(3, 1)
-    b_wait(1, 0)
-    far(1, 0)
     b_forward(1, 1)
-    b_wait(2, 0)
-    for c in range(4):
-        finish(c)
-        go(t_copy(c, tp))
+    for r in (3, 1, 2):
+        d_start(r, 1)
+    lax.fori_loop(6, 8, compressed, 0)
     b_forward(2, 1)
-    b_wait(3, 1)
-    far(3, 1)
-    b_wait(1, 1)
-    far(1, 1)
-    b_wait(2, 1)
-    for c in range(4, 7):
-        finish(c)
-        go(t_copy(c, tp))
-    finish(7)
+    for g in (0, 1):
+        for r in (0, 3, 1):
+            b_wait(r, g)
+        far_group(g)
+        b_wait(2, g)
+        for c in (4 * g, 4 * g + 2):
+            finish(c, 2)
+            for k in (c, c + 1):
+                if k < 7:
+                    go(t_copy(k, tp))
     hr[tp] = mix[7]
 
     ow_in.wait()

time: 78.4 us -> 61.9 us (0.79)
  Pallas kernels: 74.4 us -> 58 us
    pallas_call x1, Pallas kernels: 74.4 us -> 58 us  [per_device(): pl.pallas_call(kernel, in_specs=[pl.BlockSpec(memory_space=pltpu.SMEM)] +...]
where the time goes in v3:
time: 61.9 us; the launch traced here: 61.7 us
  Pallas kernels  58 us (94%)
  local copies, waits for them, and re-layouts  2.3 us (4%)
  other arithmetic  1.35 us (2%)
    pallas_call x1, Pallas kernels, per_device(): pl.pallas_call(kernel, in_specs=[pl.BlockSpec(memory_space=pltpu.SMEM)] +...  58 us
    unnamed x1, local copies, waits for them, and re-layouts  2.3 us

profile of v3, /device:TPU:1, one launch (start us, length us, event | category | flops | bytes accessed | tf_op | source)
XLA Modules:
  0.0 61.7 jit_solution(16909857023057449668)
XLA Ops:
  0.0 0.7 %fusion = (s32[8,256]{1,0:T(8,128)S(1)}, s32[8,256]{1,0:T(8,128)S(1)}) fusion(s32[1,256,8]{1,2,0:T(8,128)} %param.36, s32[256]{0:T(256)S(1)} %iota_multiply_fusion), kind=kLoop, calls=%fused_computation.5 | loop fusion | flops 10240 | bytes 25600 | tf_op jit(solution)/shard_map/shift_right_arithmetic | solution.py:492
  0.7 0.6 %select_reduce_fusion.tab = s32[16,256]{1,0:T(8,128)} fusion(s32[8,256]{1,0:T(8,128)S(1)} %get-tuple-element.6, s32[8,256]{1,0:T(8,128)S(1)} %get-tuple-element.5), kind=kLoop, calls=%fused_computation | loop fusion | flops 94208 | bytes 32768 | tf_op jit(solution)/shard_map/reduce_sum | solution.py:493
  1.4 58.0 %layer.1 = bf16[256,2048]{1,0:T(8,128)(2,1)} custom-call(s32[16,256]{1,0:T(8,128)} %select_reduce_fusion.tab, bf16[2048]{0:T(1024)(128)(2,1)} %gain_ref.1, bf16[32,64]{1,0:T(8,128)(2,1)} %bitcast.40, bf16[64,64]{1,0:T(8,128)(2,1)} %bitcast.38, bf16[32,64]{1,0:T(8,128)(2,1)} %bitcast.41, bf16[64,64]{1,0:T(8,128)(2,1)} %bitcast.39, ...), custom_call_target="tpu_custom_call" | custom-call | tf_op jit(solution)/shard_map/layer/pallas_call | solution.py:505
  59.4 2.3 %copy.23 = bf16[256,2048]{1,0:T(8,128)(2,1)} copy(bf16[256,2048]{1,0:T(8,128)(2,1)} %layer.1) | data formatting | bytes 2097152
  (1 shorter events, 0.0 us)

commit v4 on v3

--- a/solution.py
+++ b/solution.py
@@ -14,6 +14,7 @@
 TOK = 2048
 NQ = TOK // QB
 NB = TOK // SEL
+PITCH = 40
 EPS = 1e-06
 NEG = -1e30
 FLOOR = -1e20
@@ -48,10 +49,10 @@
 
 
 def kernel(
-    tab, gain_ref, ke_ref, ko_ref, ve_ref, vo_ref, fc_ref, fs_ref, sg_ref,
+    picks_ref, gain_ref, ke_ref, ko_ref, ve_ref, vo_ref, fc_ref, fs_ref, sg_ref,
     tok_hbm, wq_hbm, wck_hbm, wcv_hbm, wsk_hbm, wsv_hbm, bw_hbm, ki_hbm, vi_hbm, cc_hbm, cs_hbm, ow_hbm,
     out_hbm,
-    tok, wst, w1, wqv, bwv, w2, kiv, viv, ccv, csv, ow, inv_s, cos_s, sin_s, raw, qs, qc, gt,
+    tab, tabv, tok, wst, w1, wqv, bwv, w2, kiv, viv, ccv, csv, ow, inv_s, cos_s, sin_s, raw, qs, qc, gt,
     kvb, full1, full2, full3, inb, outb, fwd, own, sums, vtc, acc, mrow, ocmp, mix, hr, res,
     l_sem, a_send, a_recv, af_send, af_recv, s_send, s_recv, b_send, b_recv, f_send, f_recv, t_send, t_recv, o_sem,
 ):
@@ -125,6 +126,12 @@
     def af_copy(slot, part, r):
         rows = pl.ds(part * half, half)
         return remote(full[slot].at[rows], full2.at[rows], af_send.at[part], af_recv.at[part], near(r, 0))
+
+    picks = picks_ref[...]
+    code = (picks & (NB - 1)) + jnp.where(picks < 2 * lanes((8, 256)), 64, 0)
+    for span in range(16):
+        tabv[span:span + 1, :] = jnp.sum(jnp.where((picks >> 5) == span, code, 0), axis=0, keepdims=True)
+    tab_in = fetch(tabv, tab)
 
     gain = gain_ref[...].astype(F32).reshape(1, D)
     for copy in w_in:
@@ -168,38 +175,15 @@
             kvb[b] = jnp.where(low64, sel[0:64], pltpu.roll(vt, 64, 1)).astype(BF)
             kvb[b + 1] = jnp.where(low64, sel[64:128], vt).astype(BF)
             val = (proj[j * QB:(j + 1) * QB, 128:256] * scale).astype(BF).astype(F32) + embed
-            raw[part, :] = val.astype(BF).astype(F32)
+            val = val.astype(BF).astype(F32)
+            for n in range(QB // CMP):
+                spot = (t * (TILE // CMP) + j * (QB // CMP) + n) * PITCH
+                raw[spot:spot + CMP, :] = val[n * CMP:(n + 1) * CMP]
         if t % 2 == 1:
             if t == 1:
                 pl.semaphore_wait(barrier, len(peers))
             for slot, r in ((3, 1), (1, 3)):
                 go(a_copy(slot, t // 2, r))
-
-    for copy in i_in:
-        copy.wait()
-    keys, values = [], []
-    for r in range(0, CMP, 2):
-        one = raw[pl.ds(r, 64, stride=CMP), :]
-        two = raw[pl.ds(r + 1, 64, stride=CMP), :]
-        keys.append(jnp.where(low64, one, pltpu.roll(two, 64, 1)).astype(BF))
-        values.append(jnp.where(low64, pltpu.roll(one, 64, 1), two).astype(BF))
-    parts = []
-    for rows, inner, outer in ((keys, kiv, ko_ref), (values, viv, vo_ref)):
-        flat = jnp.concatenate(rows, axis=1)
-        hidden = gelu(lax.dot_general(flat, inner[...], NT, preferred_element_type=F32)).astype(BF)
-        parts.append(jnp.dot(hidden, outer[...], preferred_element_type=F32))
-    both = jnp.concatenate(parts, axis=1)
-    own[...] = jnp.where(low64, both, jnp.concatenate([both, both], axis=0).T[64:128]).astype(BF)
-    sums[0, 0] = own[...]
-
-    def s_copy(r):
-        return remote(own, sums.at[0, 4 - r], s_send.at[r - 1], s_recv.at[3 - r], near(r, 0))
-
-    def s_bundle(s):
-        return remote(sums.at[0], sums.at[4 - s], s_send.at[2 + s], s_recv.at[6 - s], near(0, s))
-
-    for r in (1, 2, 3):
-        go(s_copy(r))
 
     def dest_of(c):
         dest = 0
@@ -268,8 +252,41 @@
             b_copy(r, g, k).wait_recv()
             bf_copy(r, g, k).wait_recv()
 
-    select(0, 0)
-    select(0, 1)
+    tab_in.wait()
+    for g in (0, 1):
+        select(0, g)
+        f_start(0, g)
+    d_start(0, 0)
+    d_start(0, 1)
+
+    for copy in i_in:
+        copy.wait()
+    keys, values = [], []
+    for r in range(0, CMP, 2):
+        one = raw[pl.ds(r, 64, stride=PITCH), :]
+        two = raw[pl.ds(r + 1, 64, stride=PITCH), :]
+        keys.append(jnp.where(low64, one, pltpu.roll(two, 64, 1)).astype(BF))
+        values.append(jnp.where(low64, pltpu.roll(one, 64, 1), two).astype(BF))
+    parts = []
+    for rows, inner, outer in ((keys, kiv, ko_ref), (values, viv, vo_ref)):
+        flat = jnp.concatenate(rows, axis=1)
+        hidden = gelu(lax.dot_general(flat, inner[...], NT, preferred_element_type=F32)).astype(BF)
+        parts.append(jnp.dot(hidden, outer[...], preferred_element_type=F32))
+    both = jnp.concatenate(parts, axis=1)
+    own[...] = jnp.where(low64, both, jnp.concatenate([both, both], axis=0).T[64:128]).astype(BF)
+    sums[0, 0] = own[...]
+
+    def s_copy(r):
+        return remote(own, sums.at[0, 4 - r], s_send.at[r - 1], s_recv.at[3 - r], near(r, 0))
+
+    def s_bundle(s):
+        return remote(sums.at[0], sums.at[4 - s], s_send.at[2 + s], s_recv.at[6 - s], near(0, s))
+
+    for r in (1, 2, 3):
+        go(s_copy(r))
+
+    a_copy(3, 0, 1).wait_recv()
+    go(af_copy(3, 0, 1))
 
     for copy in q_in:
         copy.wait()
@@ -300,16 +317,24 @@
 
     queries(0)
     queries(1)
+    a_copy(1, 1, 1).wait_recv()
+    go(af_copy(1, 1, 3))
     for r in (1, 2, 3):
         s_copy(r).wait_recv()
     for s in (1, 2, 3):
         go(s_bundle(s))
-    b_start(0, 0)
-    b_start(0, 1)
-    a_copy(3, 0, 1).wait_recv()
-    go(af_copy(3, 0, 1))
     queries(2)
     queries(3)
+    b_forward(0, 0)
+    b_forward(0, 1)
+    a_copy(3, 1, 1).wait_recv()
+    a_copy(1, 0, 1).wait_recv()
+    for g in (0, 1):
+        for r in (3, 1):
+            select(r, g)
+            f_start(r, g)
+    d_start(3, 0)
+    d_start(1, 0)
 
     def values_of(blocks):
         pairs = [
@@ -361,7 +386,7 @@
     def ids_of(c0, n):
         return [(tp_at(*ORDER[c]) * 2 + k, 2 * c + k) for c in range(c0, c0 + n) for k in (0, 1)]
 
-    def far_group(g):
+    def far_loop(g, lo, hi):
         ids = ids_of(4 * g, 4)
 
         def body(n, _):
@@ -371,32 +396,34 @@
                 acc[i] = a
             return 0
 
-        lax.fori_loop(0, 3, body, 0)
-
-    def compressed(c, _):
-        q0 = dest_of(c) * 2
-        for k in (0, 1):
-            q, i = q0 + k, 2 * c + k
-            scs, ms = [], []
+        lax.fori_loop(lo, hi, body, 0)
+
+    def compressed(n, _):
+        ids = []
+        for c in (n,):
+            q0 = dest_of(c) * 2
+            ids += [(q0 + k, 2 * c + k) for k in (0, 1)]
+        scs = [
+            [jnp.dot(sums[s].reshape(256, 128), qc[q], preferred_element_type=F32) for s in range(4)] for q, _ in ids
+        ]
+        ps = []
+        for (q, _), sc in zip(ids, scs):
+            ones, ms = [], []
             m = jnp.full((1, 256), FLOOR, F32)
             for s in range(4):
-                sc = jnp.dot(sums[s].reshape(256, 128), qc[q], preferred_element_type=F32)
                 for r in range(4):
-                    one = sc[64 * r:64 * r + 64]
+                    one = sc[s][64 * r:64 * r + 64]
                     bias = jnp.where(at(r, s) < kv, 0.0, NEG)
                     if r == 0 and s == 0:
                         end = (rows_of(one.shape) + 1) * CMP - 1
                         one = jnp.where(end <= q * QB + (lanes(one.shape) & (QB - 1)), one, NEG)
                         bias = 0.0
-                    scs.append(one)
+                    ones.append(one)
                     ms.append(bias)
                     m = jnp.maximum(m, top(one) + bias)
-            total = jnp.zeros((80, 256), F32)
-            for s in range(4):
-                p = [jnp.exp(scs[4 * s + r] - (m - ms[4 * s + r])).astype(BF) for r in range(4)]
-                total += jnp.dot(
-                    vtc[:, 256 * s:256 * s + 256], jnp.concatenate(p, axis=0), preferred_element_type=F32
-                )
+            ps.append(jnp.concatenate([jnp.exp(o - (m - b)).astype(BF) for o, b in zip(ones, ms)], axis=0))
+        for (_, i), p in zip(ids, ps):
+            total = jnp.dot(vtc[...], p, preferred_element_type=F32)
             den = total[64:65]
             ocmp[i] = jnp.where(den > 0, total[0:64] / jnp.maximum(den, 1e-30), 0.0)
         return 0
@@ -419,26 +446,6 @@
 
     own_group(0)
     own_group(1)
-    a_copy(1, 1, 1).wait_recv()
-    go(af_copy(1, 1, 3))
-    for s in (1, 2, 3):
-        s_bundle(s).wait_recv()
-    for s in range(4):
-        vtc[:, 256 * s:256 * s + 256] = values_of([sums[s, r] for r in range(4)])
-    lax.fori_loop(0, 2, compressed, 0)
-    a_copy(3, 1, 1).wait_recv()
-    a_copy(1, 0, 1).wait_recv()
-    for r in (3, 1):
-        select(r, 0)
-        f_start(r, 0)
-    for r in (3, 1):
-        select(r, 1)
-        f_start(r, 1)
-    d_start(3, 0)
-    d_start(1, 0)
-    b_forward(0, 0)
-    b_forward(0, 1)
-    lax.fori_loop(2, 4, compressed, 0)
     af_copy(3, 0, 1).wait_recv()
     af_copy(1, 1, 1).wait_recv()
     for g in (0, 1):
@@ -447,18 +454,26 @@
     b_forward(3, 0)
     b_forward(1, 0)
     d_start(2, 0)
-    lax.fori_loop(4, 6, compressed, 0)
+    for s in (1, 2, 3):
+        s_bundle(s).wait_recv()
+    for s in range(4):
+        vtc[:, 256 * s:256 * s + 256] = values_of([sums[s, r] for r in range(4)])
+    lax.fori_loop(0, 2, compressed, 0)
     b_forward(2, 0)
     b_forward(3, 1)
     b_forward(1, 1)
     for r in (3, 1, 2):
         d_start(r, 1)
-    lax.fori_loop(6, 8, compressed, 0)
+    lax.fori_loop(2, 4, compressed, 0)
     b_forward(2, 1)
+    lax.fori_loop(4, 8, compressed, 0)
     for g in (0, 1):
-        for r in (0, 3, 1):
+        b_wait(0, g)
+        far_loop(g, 0, 1)
+    for g in (0, 1):
+        for r in (3, 1):
             b_wait(r, g)
-        far_group(g)
+        far_loop(g, 1, 3)
         b_wait(2, g)
         for c in (4 * g, 4 * g + 2):
             finish(c, 2)
@@ -485,14 +500,6 @@
         copy.wait()
 
 
-def pick_table(chosen):
-    picks = chosen[0].T
-    block = jnp.arange(256, dtype=jnp.int32)[None, :]
-    code = (picks & (NB - 1)) + jnp.where(picks < 2 * block, 64, 0)
-    match = (picks >> 5)[None] == jnp.arange(16, dtype=jnp.int32)[:, None, None]
-    return jnp.sum(jnp.where(match, code[None], 0), axis=1)
-
-
 def per_device(
     tokens, norm_gain, query_weight, cmp_key_weight, cmp_value_weight, sel_key_weight, sel_value_weight,
     branch_weight, key_embed, key_inner, key_outer, value_embed, value_inner, value_outer, out_weight, chosen,
@@ -504,26 +511,27 @@
     v = pltpu.VMEM
     return pl.pallas_call(
         kernel,
-        in_specs=[pl.BlockSpec(memory_space=pltpu.SMEM)] + [vm] * 8 + [hbm] * 12,
+        in_specs=[vm] * 9 + [hbm] * 12,
         out_specs=hbm,
         out_shape=jax.ShapeDtypeStruct((256, D), BF),
         scratch_shapes=[
+            pltpu.SMEM((16, 256), jnp.int32), v((16, 256), jnp.int32),
             v((TOK, D), BF), v((256, D), BF), v((256, D), BF), v((D, 128), BF), v((2, 16, D), BF), v((256, D), BF),
             v((64, D), BF), v((64, D), BF), v((32, 128), F32), v((32, 128), F32), v((1024, D), BF),
-            v((TOK, 128), F32), v((TOK, 128), F32), v((TOK, 128), F32), v((TOK, 128), F32),
+            v((TOK, 128), F32), v((TOK, 128), F32), v((TOK, 128), F32), v((64 * PITCH, 128), F32),
             v((NQ, 128, 256), BF), v((NQ, 128, 256), BF), v((NQ, 8, 128), F32),
             v((NB, SEL, 128), BF), v((NB, SEL, 128), BF), v((NB, SEL, 128), BF), v((NB, SEL, 128), BF),
             v((4, 4, NQ, SEL, 128), BF), v((4, 3, NQ, SEL, 128), BF), v((4, 2, 2, 4, SEL, 128), BF),
             v((64, 128), BF), v((4, 4, 64, 128), BF), v((80, 1024), BF),
             v((NQ, 80, 256), F32), v((NQ, 1, 256), F32), v((NQ, 64, 256), F32),
             v((8, 256, 128), BF), v((8, 256, 128), BF), v((256, D), BF),
-            dma((16,)), dma((4,)), dma((4,)), dma((2,)), dma((2,)), dma((6,)), dma((6,)),
+            dma((17,)), dma((4,)), dma((4,)), dma((2,)), dma((2,)), dma((6,)), dma((6,)),
             dma((4, 2, 4)), dma((4, 2, 4)), dma((4, 4)), dma((4, 4)), dma((8,)), dma((8,)), dma((4,)),
         ],
         compiler_params=pltpu.CompilerParams(collective_id=0, has_side_effects=True, vmem_limit_bytes=67043328),
         name="layer",
     )(
-        pick_table(chosen), norm_gain, key_embed[0], key_outer[0], value_embed[0], value_outer[0], fc, fs, sg,
+        chosen[0].T, norm_gain, key_embed[0], key_outer[0], value_embed[0], value_outer[0], fc, fs, sg,
         tokens, query_weight, cmp_key_weight.T, cmp_value_weight.T, sel_key_weight.T, sel_value_weight.T,
         branch_weight.transpose(0, 2, 1), key_inner[0].T, value_inner[0].T, cc, cs, out_weight,
     )

time: 61.9 us -> 59 us (0.953)
  Pallas kernels: 58 us -> 56.5 us
  other arithmetic: 1.35 us -> 0 us
    pallas_call x1, Pallas kernels: 58 us -> 56.5 us  [per_device(): pl.pallas_call(kernel, in_specs=[vm] * 9 + [hbm] * 12, out_specs=hbm, out...]
    shift_right_arithmetic x1 -> x0, other arithmetic: 0.7 us -> none  [pick_table(): match = (picks >> 5)[None] == jnp.arange(16, dtype=jnp.int32)[:, None, None]]
    reduce_sum x1 -> x0, other arithmetic: 0.65 us -> none  [pick_table(): return jnp.sum(jnp.where(match, code[None], 0), axis=1)]
where the time goes in v4:
time: 59 us; the launch traced here: 58.8 us
  Pallas kernels  56.5 us (96%)
  local copies, waits for them, and re-layouts  2.3 us (4%)
    pallas_call x1, Pallas kernels, per_device(): pl.pallas_call(kernel, in_specs=[vm] * 9 + [hbm] * 12, out_specs=hbm, out...  56.5 us
    unnamed x1, local copies, waits for them, and re-layouts  2.3 us

profile of v4, /device:TPU:1, one launch (start us, length us, event | category | flops | bytes accessed | tf_op | source)
XLA Modules:
  0.0 58.8 jit_solution(9854480533693850291)
XLA Ops:
  0.0 56.5 %layer.1 = bf16[256,2048]{1,0:T(8,128)(2,1)} custom-call(s32[8,256]{1,0:T(8,128)} %bitcast.27, bf16[2048]{0:T(1024)(128)(2,1)} %gain_ref.1, bf16[32,64]{1,0:T(8,128)(2,1)} %bitcast.28, bf16[64,64]{1,0:T(8,128)(2,1)} %bitcast.25, bf16[32,64]{1,0:T(8,128)(2,1)} %bitcast.29, bf16[64,64]{1,0:T(8,128)(2,1)} %bitcast.26, f32[64,128]{1,0:T(8,128)} %constant.12.clone.fc_ref, ...), custom_call_target="tpu_custom_call" | custom-call | tf_op jit(solution)/shard_map/layer/pallas_call | solution.py:512
  56.5 2.3 %copy.23 = bf16[256,2048]{1,0:T(8,128)(2,1)} copy(bf16[256,2048]{1,0:T(8,128)(2,1)} %layer.1) | data formatting | bytes 2097152

commit v5 on v4

--- a/solution.py
+++ b/solution.py
@@ -53,7 +53,7 @@
     tok_hbm, wq_hbm, wck_hbm, wcv_hbm, wsk_hbm, wsv_hbm, bw_hbm, ki_hbm, vi_hbm, cc_hbm, cs_hbm, ow_hbm,
     out_hbm,
     tab, tabv, tok, wst, w1, wqv, bwv, w2, kiv, viv, ccv, csv, ow, inv_s, cos_s, sin_s, raw, qs, qc, gt,
-    kvb, full1, full2, full3, inb, outb, fwd, own, sums, vtc, acc, mrow, ocmp, mix, hr, res,
+    kvb, full1, full2, full3, inb, outb, fwd, own, sums, vtc, acc, mrow, ocmp, mix, hr, res, part_s,
     l_sem, a_send, a_recv, af_send, af_recv, s_send, s_recv, b_send, b_recv, f_send, f_recv, t_send, t_recv, o_sem,
 ):
     full = (kvb, full1, full2, full3)
@@ -458,15 +458,15 @@
         s_bundle(s).wait_recv()
     for s in range(4):
         vtc[:, 256 * s:256 * s + 256] = values_of([sums[s, r] for r in range(4)])
-    lax.fori_loop(0, 2, compressed, 0)
+    lax.fori_loop(0, 3, compressed, 0)
     b_forward(2, 0)
     b_forward(3, 1)
     b_forward(1, 1)
     for r in (3, 1, 2):
         d_start(r, 1)
-    lax.fori_loop(2, 4, compressed, 0)
+    lax.fori_loop(3, 5, compressed, 0)
     b_forward(2, 1)
-    lax.fori_loop(4, 8, compressed, 0)
+    lax.fori_loop(5, 8, compressed, 0)
     for g in (0, 1):
         b_wait(0, g)
         far_loop(g, 0, 1)
@@ -483,14 +483,31 @@
     hr[tp] = mix[7]
 
     ow_in.wait()
-    for c in range(7):
+
+    def source(c):
         dy, dc = ORDER[c]
-        t_copy(c, tp_at((4 - dy) % 4, dc)).wait_recv()
-    x = jnp.concatenate([hr[t] for t in range(8)], axis=1)
+        return tp_at((4 - dy) % 4, dc)
+
+    def arrive(c):
+        t_copy(c, source(c)).wait_recv()
+
+    def product(cs, cols):
+        x = jnp.concatenate([hr[source(c)] for c in cs], axis=1)
+        w = jnp.concatenate([ow[pl.ds(pl.multiple_of(source(c) * 128, 128), 128), cols] for c in cs], axis=0)
+        return jnp.dot(x, w, preferred_element_type=F32)
+
+    early, late = (7, 0, 1, 2, 3), (4, 5, 6)
+    for c in early[1:]:
+        arrive(c)
+    for n in range(4):
+        cols = pl.ds(n * 512, 512)
+        part_s[:, cols] = product(early, cols)
+    for c in late:
+        arrive(c)
     outs = []
     for n in range(4):
         cols = pl.ds(n * 512, 512)
-        res[:, cols] = jnp.dot(x, ow[:, cols], preferred_element_type=F32).astype(BF)
+        res[:, cols] = (part_s[:, cols] + product(late, cols)).astype(BF)
         copy = pltpu.make_async_copy(res.at[:, cols], out_hbm.at[:, cols], o_sem.at[n])
         copy.start()
         outs.append(copy)
@@ -524,7 +541,7 @@
             v((4, 4, NQ, SEL, 128), BF), v((4, 3, NQ, SEL, 128), BF), v((4, 2, 2, 4, SEL, 128), BF),
             v((64, 128), BF), v((4, 4, 64, 128), BF), v((80, 1024), BF),
             v((NQ, 80, 256), F32), v((NQ, 1, 256), F32), v((NQ, 64, 256), F32),
-            v((8, 256, 128), BF), v((8, 256, 128), BF), v((256, D), BF),
+            v((8, 256, 128), BF), v((8, 256, 128), BF), v((256, D), BF), v((256, D), F32),
             dma((17,)), dma((4,)), dma((4,)), dma((2,)), dma((2,)), dma((6,)), dma((6,)),
             dma((4, 2, 4)), dma((4, 2, 4)), dma((4, 4)), dma((4, 4)), dma((8,)), dma((8,)), dma((4,)),
         ],

time: 59 us -> 57.7 us (0.978)
  Pallas kernels: 56.5 us -> 55.1 us
    pallas_call x1, Pallas kernels: 56.5 us -> 55.1 us  [per_device(): pl.pallas_call(kernel, in_specs=[vm] * 9 + [hbm] * 12, out_specs=hbm, out...]
where the time goes in v5:
time: 57.7 us; the launch traced here: 57.4 us
  Pallas kernels  55.1 us (95%)
  local copies, waits for them, and re-layouts  2.3 us (4%)
    pallas_call x1, Pallas kernels, per_device(): pl.pallas_call(kernel, in_specs=[vm] * 9 + [hbm] * 12, out_specs=hbm, out...  55.1 us
    unnamed x1, local copies, waits for them, and re-layouts  2.3 us

profile of v5, /device:TPU:1, one launch (start us, length us, event | category | flops | bytes accessed | tf_op | source)
XLA Modules:
  0.0 57.4 jit_solution(10646563448073680549)
XLA Ops:
  0.0 55.1 %layer.1 = bf16[256,2048]{1,0:T(8,128)(2,1)} custom-call(s32[8,256]{1,0:T(8,128)} %bitcast.27, bf16[2048]{0:T(1024)(128)(2,1)} %gain_ref.1, bf16[32,64]{1,0:T(8,128)(2,1)} %bitcast.28, bf16[64,64]{1,0:T(8,128)(2,1)} %bitcast.25, bf16[32,64]{1,0:T(8,128)(2,1)} %bitcast.29, bf16[64,64]{1,0:T(8,128)(2,1)} %bitcast.26, f32[64,128]{1,0:T(8,128)} %constant.12.clone.fc_ref, ...), custom_call_target="tpu_custom_call" | custom-call | tf_op jit(solution)/shard_map/layer/pallas_call | solution.py:529
  55.1 2.3 %copy.23 = bf16[256,2048]{1,0:T(8,128)(2,1)} copy(bf16[256,2048]{1,0:T(8,128)(2,1)} %layer.1) | data formatting | bytes 2097152

commit v6 on v5

--- a/solution.py
+++ b/solution.py
@@ -458,15 +458,15 @@
         s_bundle(s).wait_recv()
     for s in range(4):
         vtc[:, 256 * s:256 * s + 256] = values_of([sums[s, r] for r in range(4)])
-    lax.fori_loop(0, 3, compressed, 0)
+    lax.fori_loop(0, 4, compressed, 0)
     b_forward(2, 0)
     b_forward(3, 1)
     b_forward(1, 1)
     for r in (3, 1, 2):
         d_start(r, 1)
-    lax.fori_loop(3, 5, compressed, 0)
+    lax.fori_loop(4, 6, compressed, 0)
     b_forward(2, 1)
-    lax.fori_loop(5, 8, compressed, 0)
+    lax.fori_loop(6, 8, compressed, 0)
     for g in (0, 1):
         b_wait(0, g)
         far_loop(g, 0, 1)

time: 57.7 us -> 57.6 us (level)
  no operation moved by 1% of the time
where the time goes in v6:
time: 57.6 us; the launch traced here: 57.4 us
  Pallas kernels  55.1 us (96%)
  local copies, waits for them, and re-layouts  2.3 us (4%)
    pallas_call x1, Pallas kernels, per_device(): pl.pallas_call(kernel, in_specs=[vm] * 9 + [hbm] * 12, out_specs=hbm, out...  55.1 us
    unnamed x1, local copies, waits for them, and re-layouts  2.3 us

profile of v6, /device:TPU:1, one launch (start us, length us, event | category | flops | bytes accessed | tf_op | source)
XLA Modules:
  0.0 57.4 jit_solution(3407578838689659330)
XLA Ops:
  0.0 55.1 %layer.1 = bf16[256,2048]{1,0:T(8,128)(2,1)} custom-call(s32[8,256]{1,0:T(8,128)} %bitcast.27, bf16[2048]{0:T(1024)(128)(2,1)} %gain_ref.1, bf16[32,64]{1,0:T(8,128)(2,1)} %bitcast.28, bf16[64,64]{1,0:T(8,128)(2,1)} %bitcast.25, bf16[32,64]{1,0:T(8,128)(2,1)} %bitcast.29, bf16[64,64]{1,0:T(8,128)(2,1)} %bitcast.26, f32[64,128]{1,0:T(8,128)} %constant.12.clone.fc_ref, ...), custom_call_target="tpu_custom_call" | custom-call | tf_op jit(solution)/shard_map/layer/pallas_call | solution.py:529
  55.1 2.3 %copy.23 = bf16[256,2048]{1,0:T(8,128)(2,1)} copy(bf16[256,2048]{1,0:T(8,128)(2,1)} %layer.1) | data formatting | bytes 2097152
